TPU v7x, 512 devices: a whole 4x8x8 slice. The times are simulated.
512 devices in a mesh: ep: 32 (over z, x), tp: 16 (over y, core).
Axes of the slice: x: 4, y: 8, z: 8, core: 2. Of those that a mesh axis runs over, the one named last changes fastest.
Arguments:
- mixer_rows: bfloat16 [4096, 2048], P('ep'), may hold values from -40 to 40
- mixer_gain: float32 [2048], replicated, may hold values from 0.1 to 1.9
- inner_weight: bfloat16 [2048, 1024], P(None, 'tp'), may hold values from -0.125 to 0.125
- gate_in_weight: bfloat16 [2048, 1024], P(None, 'tp'), may hold values from -0.125 to 0.125
- gate_out_weight: bfloat16 [2048, 1024], P(None, 'tp'), may hold values from -0.125 to 0.125
- conv_taps: float32 [3, 1024], P(None, 'tp'), may hold values from -3.5 to 3.5
- mixer_out_weight: bfloat16 [1024, 2048], P('tp'), may hold values from -0.1875 to 0.1875
- routed_rows: bfloat16 [8192, 2048], P('ep'), may hold values from -40 to 40
- routed_gain: float32 [2048], replicated, may hold values from 0.1 to 1.9
- route_ids: int32 [8192, 2], P('ep'), may hold values from 0 to 31, all different within a row; in each aligned block of 256 rows (0 to 255, 256 to 511, ...) at most 32 rows name the same one
- route_weights: float32 [8192, 2], P('ep'), may hold values from 0.25 to 1
- expert_gate: bfloat16 [32, 2048, 2048], P('ep', None, 'tp'), may hold values from -0.125 to 0.125
- expert_up: bfloat16 [32, 2048, 2048], P('ep', None, 'tp'), may hold values from -0.125 to 0.125
- expert_down: bfloat16 [32, 2048, 2048], P('ep', 'tp'), may hold values from -0.125 to 0.125
Outputs:
- mixer_output: bfloat16 [4096, 2048], P('ep')
- routed_output: bfloat16 [8192, 2048], P('ep')
Inputs may be any that keep to these rules, and one draw needn't show every extreme that they name: `route_ids`: within each aligned block of 256 tokens, no expert is named by more than 32 choices, a bound that some block reaches; a token's 2 experts differ.
All inputs are finite; a program needn't handle non-finite values.
Results may differ from a plain program's by a relative error of at most 0.019.
Values may be sent and summed in bfloat16 or wider, within the bound.
A program may use at most 64 MiB of HBM per device.

v0:
```python
import jax
import jax.numpy as jnp
from jax import lax
from jax.sharding import PartitionSpec as P


def shifted(value, axis, steps):
    count = lax.axis_size(axis)
    initial, last = (max(0, -steps), min(count, count - steps))
    return lax.ppermute(value, axis, [(source, source + steps) for source in range(initial, last)])


def packed_total(arrays, axis):
    ends = [0]
    for a in arrays:
        ends.append(ends[-1] + a.size)
    so_far = lax.psum(jnp.concatenate([a.ravel() for a in arrays]), axis)
    return tuple((so_far[b:e].reshape(a.shape) for a, b, e in zip(arrays, ends, ends[1:])))


def rms_scale(row_block, gain_row):
    values = row_block.astype(jnp.float32)
    scaled = values * lax.rsqrt(jnp.mean(values * values, axis=-1, keepdims=True) + 1e-06)
    return (scaled * gain_row).astype(jnp.bfloat16)


def on_device(
    mixer_rows,
    mixer_gain,
    inner_weight,
    gate_in_weight,
    gate_out_weight,
    conv_taps,
    mixer_out_weight,
    routed_rows,
    routed_gain,
    route_ids,
    route_weights,
    expert_gate,
    expert_up,
    expert_down,
):
    normed = rms_scale(mixer_rows, mixer_gain)
    inner_proj = jnp.dot(normed, inner_weight, preferred_element_type=jnp.float32)
    gate_in = jnp.dot(normed, gate_in_weight, preferred_element_type=jnp.float32)
    conv_input = (gate_in * inner_proj).astype(jnp.bfloat16)
    gate_out = jnp.dot(normed, gate_out_weight, preferred_element_type=jnp.float32)
    tap_total = conv_taps.shape[0]
    rim_rows = tap_total - 1
    earlier_rows = shifted(conv_input[conv_input.shape[0] - rim_rows :], "ep", 1)
    extended = jnp.concatenate([earlier_rows, conv_input], axis=0).astype(jnp.float32)
    length = conv_input.shape[0]
    conv_out = jnp.zeros(conv_input.shape, jnp.float32)
    for tap_index in range(tap_total):
        conv_out = conv_out + conv_taps[tap_index] * extended[tap_index : tap_index + length]
    gated_conv = (gate_out * conv_out).astype(jnp.bfloat16)
    mixer_terms = jnp.dot(gated_conv, mixer_out_weight, preferred_element_type=jnp.float32)
    routed_normed = rms_scale(routed_rows, routed_gain)
    experts = lax.axis_size("ep")
    groups = lax.axis_size("tp")
    column = lax.axis_index("tp")
    tok_count, pick_count = route_ids.shape
    model_width = routed_rows.shape[1]
    capacity = 2 * tok_count * pick_count // experts
    share_rows = capacity // groups
    flat_ids = route_ids.reshape(-1)
    onehot = (flat_ids[:, None] == jnp.arange(experts, dtype=jnp.int32)[None, :]).astype(jnp.int32)
    slot_rank = jnp.sum((jnp.cumsum(onehot, axis=0) - onehot) * onehot, axis=1)
    slot_number = slot_rank * experts + flat_ids
    owners = jnp.arange(tok_count * pick_count, dtype=jnp.int32) // pick_count
    matches = slot_number[None, :] == jnp.arange(capacity * experts, dtype=jnp.int32)[:, None]
    token_table = jnp.where(
        jnp.any(matches, axis=1), jnp.sum(jnp.where(matches, owners[None, :], 0), axis=1), tok_count
    )
    padded_rows = jnp.concatenate(
        [routed_normed, jnp.zeros((1, model_width), jnp.bfloat16)], axis=0
    )
    table_share = lax.dynamic_slice_in_dim(
        token_table.reshape(capacity, experts), column * share_rows, share_rows, 0
    )
    outgoing = jnp.take(padded_rows, table_share.reshape(-1), axis=0).reshape(
        share_rows, experts, model_width
    )
    arrived = lax.all_to_all(outgoing, "ep", split_axis=1, concat_axis=1, tiled=True)
    incoming = lax.all_gather(arrived, "tp", axis=0, tiled=True)
    slot_rows = incoming.reshape(capacity * experts, model_width)
    gate_act = jnp.dot(slot_rows, expert_gate[0], preferred_element_type=jnp.float32)
    up_act = jnp.dot(slot_rows, expert_up[0], preferred_element_type=jnp.float32)
    hidden = (jax.nn.silu(gate_act) * up_act).astype(jnp.bfloat16)
    summed = lax.psum_scatter(
        jnp.dot(hidden, expert_down[0], preferred_element_type=jnp.float32).astype(jnp.bfloat16),
        "tp",
        scatter_dimension=0,
        tiled=True,
    )
    returned = lax.all_to_all(
        summed.reshape(share_rows, experts, model_width),
        "ep",
        split_axis=1,
        concat_axis=1,
        tiled=True,
    )
    flat_back = jnp.concatenate(
        [
            returned.reshape(share_rows * experts, model_width),
            jnp.zeros((1, model_width), jnp.bfloat16),
        ],
        axis=0,
    )
    local_slot = jnp.where(
        slot_rank // share_rows == column,
        (slot_rank - column * share_rows) * experts + flat_ids,
        share_rows * experts,
    )
    contrib = (
        jnp.take(flat_back, local_slot, axis=0).astype(jnp.float32)
        * route_weights.reshape(-1)[:, None]
    )
    routed_terms = jnp.sum(contrib.reshape(tok_count, pick_count, model_width), axis=1)
    mixer_total, routed_total = tuple(
        (
            part.astype(jnp.float32)
            for part in packed_total(
                (mixer_terms.astype(jnp.bfloat16), routed_terms.astype(jnp.bfloat16)), "tp"
            )
        )
    )
    return (mixer_total.astype(jnp.bfloat16), routed_total.astype(jnp.bfloat16))


def solution(mesh):
    return jax.shard_map(
        on_device,
        mesh=mesh,
        in_specs=(
            P("ep", None),
            P(),
            P(None, "tp"),
            P(None, "tp"),
            P(None, "tp"),
            P(None, "tp"),
            P("tp", None),
            P("ep", None),
            P(),
            P("ep", None),
            P("ep", None),
            P("ep", None, "tp"),
            P("ep", None, "tp"),
            P("ep", "tp", None),
        ),
        out_specs=(P("ep", None), P("ep", None)),
        check_vma=False,
    )
```

profile of v0, /device:TPU:1, one launch (start us, length us, event | category | flops | bytes accessed | tf_op | source)
XLA Modules:
  0.0 321.4 jit_solution(4402862292982536007)
XLA Ops:
  7.2 0.9 copy.70
  8.5 1.2 reduce-window.6
  10.8 1.5 fusion
  12.4 1.0 fusion.2
  14.6 24.8 %all_to_all.10 = bf16[2,32,2048]{2,0,1:T(2,128)(2,1)S(1)} all-to-all(bf16[2,32,2048]{2,0,1:T(2,128)(2,1)S(1)} %broadcast_select_fusion.1), channel_id=1, replica_groups=mesh['ep'=32,'tp'=16] {'ep'}, dimensions={1} | all-to-all | bytes 524288 | tf_op jit(solution)/shard_map/all_to_all | solution.py:84
  40.3 42.1 %all-gather.2.cloned.1.call-done = bf16[32,32,2048]{2,1,0:T(8,128)(2,1)} async-done(((bf16[2,32,2048]{2,1,0:T(8,128)(2,1)}), bf16[32,32,2048]{2,1,0:T(8,128)(2,1)}) %all-gather.2.cloned.1.call-update) | async-done | bytes 4194320 | tf_op jit(solution)/shard_map/all_gather | solution.py:85
  82.4 3.5 %fusion.14 = f32[1024,128]{1,0:T(8,128)S(1)} fusion(bf16[1024,2048]{1,0:T(8,128)(2,1)} %bitcast.56, bf16[1,2048,128]{2,1,0:T(8,128)(2,1)S(1)} %copy-done.3), kind=kOutput, calls=%fused_computation.30 | convolution fusion | flops 536870912 | bytes 5242880 | tf_op jit(solution)/shard_map/dot_general | solution.py:87
  86.0 8.5 %convolution_convert_fusion = bf16[1024,2048]{1,0:T(8,128)(2,1)} fusion(bf16[1024,2048]{1,0:T(8,128)(2,1)} %bitcast.57, bf16[1,128,2048]{2,1,0:T(8,128)(2,1)S(1)} %copy-done, bf16[1,2048,128]{2,1,0:T(8,128)(2,1)S(1)} %copy-done.4, f32[1024,128]{1,0:T(8,128)S(1)} %fusion.14), kind=kOutput, calls=%fused_computation.4 | convolution fusion | flops 1076625408 | bytes 9961472 | tf_op jit(solution)/shard_map/dot_general | solution.py:91
  94.5 1.0 copy-done.2
  96.5 3.1 collective-permute-start
  100.1 56.6 %reduce-scatter.2.cloned.1.call-done = bf16[64,2048]{1,0:T(8,128)(2,1)} async-done(((bf16[1024,2048]{1,0:T(8,128)(2,1)}), bf16[64,2048]{1,0:T(8,128)(2,1)}) %reduce-scatter.2.cloned.1.call-update) | async-done | bytes 262160 | tf_op jit(solution)/shard_map/reduce_scatter | solution.py:90
  156.7 1.9 copy.82
  158.6 9.1 %all-to-all-start.1 = ((bf16[2,32,2048]{2,0,1:T(2,128)(2,1)}), bf16[2,32,2048]{2,0,1:T(2,128)(2,1)S(1)}, u32[]{:S(2)}, u32[]{:S(2)}) async-start(bf16[2,32,2048]{2,0,1:T(2,128)(2,1)} %copy.82), calls=%async_computation.2 | async-start | bytes 524288 | tf_op jit(solution)/shard_map/all_to_all | solution.py:96
  168.1 0.8 copy.85
  169.0 0.9 fusion.4
  170.1 8.1 %all-to-all-done.1 = bf16[2,32,2048]{2,0,1:T(2,128)(2,1)S(1)} async-done(((bf16[2,32,2048]{2,0,1:T(2,128)(2,1)}), bf16[2,32,2048]{2,0,1:T(2,128)(2,1)S(1)}, u32[]{:S(2)}, u32[]{:S(2)}) %all-to-all-start.1) | async-done | bytes 262176 | tf_op jit(solution)/shard_map/all_to_all | solution.py:96
  178.3 2.5 gather_fusion.1
  180.8 2.7 gather.15
  183.4 9.9 %multiply_reduce_fusion = bf16[256,2048]{1,0:T(8,128)(2,1)S(1)} fusion(bf16[256,2,2048]{2,1,0:T(2,128)(2,1)} %gather.15, pred[256,2]{1,0:T(8,128)(4,1)S(1)} %copy.78, f32[256,2]{1,0:T(8,128)S(1)} %copy-done.5), kind=kLoop, calls=%fused_computation.2 | loop fusion | flops 3670016 | bytes 3148288 | tf_op jit(solution)/shard_map/reduce_sum | solution.py:119
  193.5 1.3 pad_maximum_fusion
  194.8 116.5 %all-reduce.4.cloned.1.call-done = bf16[786432]{0:T(1024)(128)(2,1)} async-done(((bf16[786432]{0:T(1024)(128)(2,1)}), bf16[786432]{0:T(1024)(128)(2,1)}) %all-reduce.4.cloned.1.call-update) | async-done | bytes 1572880 | tf_op jit(solution)/shard_map/psum | solution.py:17
  311.4 1.2 slice-done
  312.6 1.3 slice.65
  313.8 1.0 slice.63
  (77 shorter events, 6.0 us)
Async XLA Ops:
  7.2 78.8 %copy-start = (bf16[1,128,2048]{2,1,0:T(8,128)(2,1)S(1)}, bf16[1,128,2048]{2,1,0:T(8,128)(2,1)}, u32[]{:S(2)}) copy-start(bf16[1,128,2048]{2,1,0:T(8,128)(2,1)} %param.27) | copy-start | bytes 1572868
  7.2 5.3 %copy-start.1 = (bf16[256,2048]{1,0:T(8,128)(2,1)S(1)}, bf16[256,2048]{1,0:T(8,128)(2,1)}, u32[]{:S(2)}) copy-start(bf16[256,2048]{1,0:T(8,128)(2,1)} %param.21) | copy-start | bytes 3145732
  7.2 75.2 %all-gather.2.cloned.1.call-start = ((), (), s32[]{:S(2)}) async-start(), calls=%async_computation.3 | async-start | bytes 4456448 | tf_op jit(solution)/shard_map/all_gather | solution.py:85
  13.5 68.9 %copy-start.3 = (bf16[1,2048,128]{2,1,0:T(8,128)(2,1)S(1)}, bf16[1,2048,128]{2,1,0:T(8,128)(2,1)}, u32[]{:S(2)}) copy-start(bf16[1,2048,128]{2,1,0:T(8,128)(2,1)} %param.25) | copy-start | bytes 1572868
  40.3 116.4 %reduce-scatter.2.cloned.1.call-start = ((), (), s32[]{:S(2)}) async-start(), calls=%async_computation.4 | async-start | bytes 4456448 | tf_op jit(solution)/shard_map/reduce_scatter | solution.py:90
  82.4 3.5 %copy-start.4 = (bf16[1,2048,128]{2,1,0:T(8,128)(2,1)S(1)}, bf16[1,2048,128]{2,1,0:T(8,128)(2,1)}, u32[]{:S(2)}) copy-start(bf16[1,2048,128]{2,1,0:T(8,128)(2,1)} %param.26) | copy-start | bytes 1572868
  94.4 1.0 copy-start.2
  94.4 1.3 copy-start.8
  94.4 1.3 copy-start.12
  94.4 1.7 copy-start.13
  95.5 4.5 %copy-start.9 = (s32[256,2]{0,1:T(2,128)S(1)}, s32[256,2]{0,1:T(2,128)}, u32[]{:S(2)}) copy-start(s32[256,2]{0,1:T(2,128)} %param.23) | copy-start | bytes 6148
  95.5 72.4 %copy-start.11 = (f32[3,64]{1,0:T(4,128)S(1)}, f32[3,64]{1,0:T(4,128)}, u32[]{:S(2)}) copy-start(f32[3,64]{1,0:T(4,128)} %param.19) | copy-start | bytes 2308
  95.5 72.7 %copy-start.10 = (f32[256,2]{0,1:T(2,128)S(1)}, f32[256,2]{0,1:T(2,128)}, u32[]{:S(2)}) copy-start(f32[256,2]{0,1:T(2,128)} %param.24) | copy-start | bytes 6148
  95.7 73.4 %copy-start.6 = (bf16[64,2048]{1,0:T(8,128)(2,1)S(1)}, bf16[64,2048]{1,0:T(8,128)(2,1)}, u32[]{:S(2)}) copy-start(bf16[64,2048]{1,0:T(8,128)(2,1)} %param.20) | copy-start | bytes 786436
  95.7 73.4 %copy-start.7 = (bf16[2048,64]{0,1:T(8,128)(2,1)S(1)}, bf16[2048,64]{0,1:T(8,128)(2,1)}, u32[]{:S(2)}) copy-start(bf16[2048,64]{0,1:T(8,128)(2,1)} %param.18) | copy-start | bytes 786436
  96.5 72.4 %collective-permute-start = (bf16[2,64]{0,1:T(8,128)(2,1)S(1)}, bf16[2,64]{0,1:T(8,128)(2,1)S(1)}, u32[]{:S(2)}, u32[]{:S(2)}) collective-permute-start(bf16[2,64]{0,1:T(8,128)(2,1)S(1)} %slice.70), channel_id=1, source_target_pairs={{0,16},{16,32},{32,48},{48,64},{64,80},{80,96},{96,112},{112,128},... | collective-permute-start | bytes 776 | tf_op jit(solution)/shard_map/ppermute | solution.py:10
  158.6 19.6 %all-to-all-start.1 = ((bf16[2,32,2048]{2,0,1:T(2,128)(2,1)}), bf16[2,32,2048]{2,0,1:T(2,128)(2,1)S(1)}, u32[]{:S(2)}, u32[]{:S(2)}) async-start(bf16[2,32,2048]{2,0,1:T(2,128)(2,1)} %copy.82), calls=%async_computation.2 | async-start | bytes 524288 | tf_op jit(solution)/shard_map/all_to_all | solution.py:96
  167.7 143.7 %all-reduce.4.cloned.1.call-start = ((), (), s32[]{:S(2)}) async-start(), calls=%async_computation.5 | async-start | bytes 3145728 | tf_op jit(solution)/shard_map/psum | solution.py:17
  180.8 2.7 copy-start.5
  311.3 1.2 slice-start
  312.6 1.3 slice-start.1
Sparse Core Ops, SparseCore 0:
  40.4 42.0 all-gather.1
  94.6 62.0 reduce-scatter.1
  194.9 116.3 all-reduce.3
where the time goes:
time: 322 us; the launch traced here: 321 us
  waiting for transfers between devices  223 us (69%)
  blocking collectives  24.8 us (8%)
  local copies, waits for them, and re-layouts  16.8 us (5%)
  other arithmetic  16.3 us (5%)
  between operations  14.1 us (4%)
  matrix products  13.6 us (4%)
  starting transfers between devices  12.5 us (4%)
    psum x1, waiting for transfers between devices, packed_total(): so_far = lax.psum(jnp.concatenate([a.ravel() for a in arrays]), axis)  117 us
    reduce_scatter x1, waiting for transfers between devices, on_device(): lax.psum_scatter(jnp.dot(hidden, expert_down[0], preferred_element_type=j...  56.6 us
    all_gather x1, waiting for transfers between devices, on_device(): incoming = lax.all_gather(arrived, 'tp', axis=0, tiled=True)  42.1 us
    all_to_all x1, blocking collectives, on_device(): lax.all_to_all(outgoing, 'ep', split_axis=1, concat_axis=1, tiled=True)  24.8 us
    reduce_sum x1, other arithmetic, on_device(): jnp.sum(contrib.reshape(tok_count, pick_count, model_width), axis=1)  9.87 us
    all_to_all x1, starting transfers between devices, on_device(): lax.all_to_all(summed.reshape(share_rows, experts, model_width), 'ep', sp...  9.09 us
    dot_general x1, matrix products, on_device(): jnp.dot(hidden, expert_down[0], preferred_element_type=jnp.float32)  8.47 us
    all_to_all x1, waiting for transfers between devices, on_device(): lax.all_to_all(summed.reshape(share_rows, experts, model_width), 'ep', sp...  8.08 us
  transfers between devices with their start and end apart: 5, of which 4 were waited for; matrix products, arithmetic and copies ran while one was open for 2% of the time, Pallas kernels for 0%

commit v1 on v0

v1 whole, which is shorter than its diff:
```python
import functools

import jax
import jax.numpy as jnp
from jax import lax
from jax.experimental import pallas as pl
from jax.experimental.pallas import tpu as pltpu
from jax.sharding import PartitionSpec as P

MESH = pl.DeviceIdType.MESH
BF = jnp.bfloat16
F32 = jnp.float32
EPS = 1e-06


def dot(a, b):
    return jnp.dot(a, b, preferred_element_type=F32)


def kernel(
    E,
    Y,
    CAP,
    mrows_hbm,
    mgain,
    win_hbm,
    wgi_hbm,
    wgo_hbm,
    taps,
    wmo_hbm,
    rrows_hbm,
    rgain,
    ids_ref,
    rw_ref,
    eg_hbm,
    eu_hbm,
    ed_hbm,
    mout,
    rout,
    mrows,
    mn,
    win,
    wgi,
    wgo,
    wmo,
    rrows,
    nrm,
    wgu,
    wd,
    slots,
    xs,
    xb,
    acc,
    hid,
    sbuf,
    rbuf,
    fin,
    ret,
    whi,
    wlo,
    ci,
    halo,
    ext,
    go,
    gsc,
    gpart,
    l_sem,
    wt_s,
    wt_r,
    a2a_s,
    a2a_r,
    halo_s,
    halo_r,
    g_s,
    g_r,
    ag_s,
    ag_r,
    rs_s,
    rs_r,
    ret_s,
    ret_r,
    mg_s,
    mg_r,
    md_s,
    md_r,
    rg_s,
    rg_r,
    rd_s,
    rd_r,
):
    S = Y // 2
    c = lax.axis_index("ep")
    t = lax.axis_index("tp")
    y = t // 2
    k = t % 2
    half_c = c // 2
    active = k == c % 2
    M, D = mn.shape
    T = nrm.shape[0]
    CW = D // Y
    NS = E * CAP
    R = NS // 2
    R2 = R // 2
    MH = M // 2
    MQ = M // 4
    HC = gsc.shape[0] and win.shape[1]
    partner = (c, y * 2 + 1 - k)
    ring = [(c, ((y + 1) % Y) * 2 + k), (c, ((y + Y - 1) % Y) * 2 + k)]
    sign = [1, -1]

    def remote(src, dst, ss, rs, dev):
        return pltpu.make_async_remote_copy(
            src_ref=src, dst_ref=dst, send_sem=ss, recv_sem=rs, device_id=dev, device_id_type=MESH
        )

    barrier = pltpu.get_barrier_semaphore()

    def greet(i, carry):
        pl.semaphore_signal(barrier, inc=1, device_id=((c + i) % E, t), device_id_type=MESH)
        return carry

    for dev in (partner, ring[0], ring[1]):
        pl.semaphore_signal(barrier, inc=1, device_id=dev, device_id_type=MESH)
    lax.fori_loop(1, E, greet, 0)

    FW = eg_hbm.shape[2]
    loads = [
        pltpu.make_async_copy(rrows_hbm, rrows, l_sem.at[0]),
        pltpu.make_async_copy(mrows_hbm, mrows, l_sem.at[1]),
        pltpu.make_async_copy(win_hbm, win, l_sem.at[2]),
        pltpu.make_async_copy(wgi_hbm, wgi, l_sem.at[3]),
        pltpu.make_async_copy(wgo_hbm, wgo, l_sem.at[4]),
        pltpu.make_async_copy(eg_hbm.at[0], wgu.at[:, pl.ds(0, FW)], l_sem.at[5]),
        pltpu.make_async_copy(eu_hbm.at[0], wgu.at[:, pl.ds(2 * FW, FW)], l_sem.at[6]),
        pltpu.make_async_copy(ed_hbm.at[0], wd.at[pl.ds(0, FW), :], l_sem.at[7]),
        pltpu.make_async_copy(wmo_hbm, wmo.at[pl.ds(0, HC), :], l_sem.at[8]),
    ]
    for one in loads:
        one.start()

    def slot_numbers():
        ids = ids_ref[...]
        lane = lax.broadcasted_iota(jnp.int32, (T, 128), 1)
        hit0 = lane == ids[:, 0:1]
        hit1 = lane == ids[:, 1:2]
        named = jnp.where(hit0 | hit1, 1.0, 0.0).astype(BF)
        r = lax.broadcasted_iota(jnp.int32, (T, T), 0)
        q = lax.broadcasted_iota(jnp.int32, (T, T), 1)
        lower = jnp.where(r > q, 1.0, 0.0).astype(BF)
        before = dot(lower, named)
        rank0 = jnp.sum(jnp.where(hit0, before, 0.0), axis=1, keepdims=True)
        rank1 = jnp.sum(jnp.where(hit1, before, 0.0), axis=1, keepdims=True)
        s0 = ids[:, 0:1].astype(F32) * CAP + rank0
        s1 = ids[:, 1:2].astype(F32) * CAP + rank1
        diag = r == q
        row0 = jnp.sum(jnp.where(diag, s0, 0.0), axis=0, keepdims=True)
        row1 = jnp.sum(jnp.where(diag, s1, 0.0), axis=0, keepdims=True)
        return s0, s1, row0, row1

    cols_y = pl.ds(pl.multiple_of(y * CW, CW), CW)

    def norm_routed():
        step = 32

        def body(i, carry):
            rows = pl.ds(pl.multiple_of(i * step, step), step)
            v = rrows[rows, :].astype(F32)
            scale = lax.rsqrt(jnp.mean(v * v, axis=-1, keepdims=True) + EPS)
            part = rrows[rows, cols_y].astype(F32)
            nrm[rows, :] = (part * scale * rgain[:, cols_y]).astype(BF)
            return carry

        lax.fori_loop(0, T // step, body, 0)

    loads[0].wait()

    CH = NS // 4
    EC = E // 4

    def dispatch(e):
        return remote(
            xs.at[pl.ds(pl.multiple_of(e * CAP, CAP), CAP), :],
            xb.at[y, pl.ds(pl.multiple_of(half_c * CAP, CAP), CAP), :],
            a2a_s.at[e],
            a2a_r.at[half_c],
            (e, t),
        )

    @pl.when(active)
    def _():
        s0, s1, row0, row1 = slot_numbers()
        slots[0] = jnp.broadcast_to(s0, (T, 128))
        slots[1] = jnp.broadcast_to(s1, (T, 128))
        norm_routed()
        row0 = row0.astype(jnp.int32)
        row1 = row1.astype(jnp.int32)

        def select(i, carry):
            first = ((c // EC + i) % 4) * CH
            number = lax.broadcasted_iota(jnp.int32, (CH, T), 0) + first
            pick = jnp.where((number == row0) | (number == row1), 1.0, 0.0).astype(BF)
            xs[pl.ds(pl.multiple_of(first, CH), CH), :] = dot(pick, nrm[...]).astype(BF)
            return carry

        lax.fori_loop(0, 4, select, 0)

    pl.semaphore_wait(barrier, E + 2)

    @pl.when(active)
    def _():
        def send(i, carry):
            dispatch((c + i) % E).start()
            return carry

        lax.fori_loop(1, E, send, 0)
        xb[y, pl.ds(pl.multiple_of(half_c * CAP, CAP), CAP), :] = xs[
            pl.ds(pl.multiple_of(c * CAP, CAP), CAP), :
        ]

    weights = [
        remote(eg_hbm.at[0], wgu.at[:, pl.ds(FW, FW)], wt_s.at[0], wt_r.at[0], partner),
        remote(eu_hbm.at[0], wgu.at[:, pl.ds(3 * FW, FW)], wt_s.at[1], wt_r.at[1], partner),
        remote(ed_hbm.at[0], wd.at[pl.ds(FW, FW), :], wt_s.at[2], wt_r.at[2], partner),
        remote(wmo_hbm, wmo.at[pl.ds(HC, HC), :], wt_s.at[3], wt_r.at[3], partner),
    ]
    for one in weights:
        one.start()

    for i in range(1, 5):
        loads[i].wait()

    def norm_mixer(i, carry):
        rows = pl.ds(pl.multiple_of(i * 16, 16), 16)
        v = mrows[rows, :].astype(F32)
        scale = lax.rsqrt(jnp.mean(v * v, axis=-1, keepdims=True) + EPS)
        mn[rows, :] = (v * scale * mgain[...]).astype(BF)
        return carry

    lax.fori_loop(0, M // 16, norm_mixer, 0)
    normed = mn[...]
    inner = dot(normed, win[...])
    gate_in = dot(normed, wgi[...])
    go[:, 0:HC] = dot(normed, wgo[...])
    ci[...] = jnp.zeros(ci.shape, BF)
    ci[:, 0:HC] = (gate_in * inner).astype(BF)
    send_halo = remote(ci.at[pl.ds(M - 16, 16), :], halo, halo_s, halo_r, ((c + 1) % E, t))
    send_halo.start()

    @pl.when(active)
    def _():
        for i in range(4):
            number = lax.broadcasted_iota(jnp.int32, (T, CH), 1) + i * CH
            s0 = slots[0][:, 0:1].astype(jnp.int32)
            s1 = slots[1][:, 0:1].astype(jnp.int32)
            w = jnp.where(number == s0, rw_ref[:, 0:1], 0.0) + jnp.where(
                number == s1, rw_ref[:, 1:2], 0.0
            )
            top = w.astype(BF)
            whi[:, i * CH : (i + 1) * CH] = top
            wlo[:, i * CH : (i + 1) * CH] = (w - top.astype(F32)).astype(BF)

    def ag(d, s, h):
        blk = (y + Y - sign[d] * (s - 1)) % Y
        ref = xb.at[blk, pl.ds(h * R2, R2), :]
        return remote(ref, ref, ag_s.at[d, s - 1, h], ag_r.at[d, s - 1, h], ring[d])

    def ag_wait(d, s, h):
        blk = (y + Y - sign[d] * s) % Y
        ref = xb.at[blk, pl.ds(h * R2, R2), :]
        remote(ref, ref, ag_s.at[d, s - 1, h], ag_r.at[d, s - 1, h], ring[d]).wait_recv()

    def gate_up(blk, h):
        return dot(
            xb[blk, h * R2 : (h + 1) * R2, :], wgu[pl.ds(pl.multiple_of(blk * CW, CW), CW), :]
        )

    def arrived(i, carry):
        @pl.when(jnp.logical_not(active & (i == half_c)))
        def _():
            remote(
                xs.at[pl.ds(0, CAP), :],
                xb.at[y, pl.ds(pl.multiple_of(i * CAP, CAP), CAP), :],
                a2a_s.at[0],
                a2a_r.at[i],
                (c, t),
            ).wait_recv()

        return carry

    for s in range(1, S + 2):
        for h in range(2):
            if s == 1:
                lax.fori_loop(h * (E // 4), (h + 1) * (E // 4), arrived, 0)
            for d in range(2):
                if s > 1 and (s - 1 < S or h == d):
                    ag_wait(d, s - 1, h)
                if s <= S and (s < S or h == d):
                    ag(d, s, h).start()
            if s == 1 and h == 0:
                loads[5].wait()
                loads[6].wait()
                weights[0].wait_recv()
                weights[1].wait_recv()
            if s == 1:
                acc[h] = gate_up(y, h)
            elif s <= S:
                acc[h] += gate_up((y + s - 1) % Y, h) + gate_up((y + Y - s + 1) % Y, h)
            else:
                both = acc[h] + gate_up((y + S) % Y, h)
                g = both[:, 0 : 2 * FW]
                hid[h] = (g / (1.0 + jnp.exp(-g)) * both[:, 2 * FW :]).astype(BF)
        if s == 1:
            send_halo.wait_recv()
            ext[0:16, :] = jnp.where(c > 0, halo[...].astype(F32), 0.0)
            ext[16:, :] = ci[...].astype(F32)
            conv = taps[0:1, :] * ext[14 : 14 + M, 0:HC]
            conv = conv + taps[1:2, :] * ext[15 : 15 + M, 0:HC]
            conv = conv + taps[2:3, :] * ext[16 : 16 + M, 0:HC]
            gsc[...] = jnp.zeros(gsc.shape, BF)
            gsc[:, 0:HC] = (go[:, 0:HC] * conv).astype(BF)
            send_g = remote(
                gsc.at[pl.ds(pl.multiple_of((1 - k) * MH, MH), MH), :], gpart, g_s, g_r, partner
            )
            send_g.start()

    loads[7].wait()
    loads[8].wait()
    weights[2].wait_recv()
    weights[3].wait_recv()
    send_g.wait_recv()

    def partial(h, dest):
        cols = pl.ds(pl.multiple_of(dest * CW, CW), CW)
        mine = gsc[pl.ds(pl.multiple_of(k * MH + h * MQ, MQ), MQ), :]
        other = gpart[h * MQ : (h + 1) * MQ, :]
        return dot(hid[h], wd[:, cols]), dot(mine[:, 0:HC], wmo[0:HC, cols]) + dot(
            other[:, 0:HC], wmo[HC:, cols]
        )

    def rs(d, s, h):
        return remote(
            sbuf.at[d, s - 1, h], rbuf.at[d, s - 1, h], rs_s.at[d, s - 1, h], rs_r.at[d, s - 1, h], ring[d]
        )

    for s in range(1, S + 1):
        for h in range(2):
            for d in range(2):
                if s == 1 and h != d:
                    continue
                a, b = partial(h, (y + Y + sign[d] * (S + 1 - s)) % Y)
                if s > 2 or (s == 2 and h == d):
                    rs(d, s - 1, h).wait_recv()
                    a = a + rbuf[d, s - 2, h, 0:R2, :].astype(F32)
                    b = b + rbuf[d, s - 2, h, R2:, :].astype(F32)
                sbuf[d, s - 1, h, 0:R2, :] = a.astype(BF)
                sbuf[d, s - 1, h, R2:, :] = b.astype(BF)
                rs(d, s, h).start()

    def giving(i):
        return remote(
            fin.at[pl.ds(pl.multiple_of(i * CAP, CAP), CAP), :],
            ret.at[pl.ds(pl.multiple_of(c * CAP, CAP), CAP), :],
            ret_s.at[i],
            ret_r.at[c],
            (2 * i + k, t),
        )

    def give(i, carry):
        @pl.when(2 * i + k != c)
        def _():
            giving(i).start()

        return carry

    for h in range(2):
        a, b = partial(h, y)
        for d in range(2):
            rs(d, S, h).wait_recv()
            a = a + rbuf[d, S - 1, h, 0:R2, :].astype(F32)
            b = b + rbuf[d, S - 1, h, R2:, :].astype(F32)
        fin[h * R2 : (h + 1) * R2, :] = a.astype(BF)
        mout[pl.ds(pl.multiple_of(k * MH + h * MQ, MQ), MQ), cols_y] = b.astype(BF)
        lax.fori_loop(h * (E // 4), (h + 1) * (E // 4), give, 0)

    def block(rel):
        return pl.ds(pl.multiple_of(((y + Y + rel) % Y) * CW, CW), CW)

    def mixer_piece(core, rel, h):
        if h is None:
            return mout.at[pl.ds(pl.multiple_of(core * MH, MH), MH), block(rel)]
        return mout.at[pl.ds(pl.multiple_of(core * MH + h * MQ, MQ), MQ), block(rel)]

    def mg(d, s, incoming):
        rel = -sign[d] * (s if incoming else s - 1)
        ref = mixer_piece(k, rel, None if s < S else d)
        return remote(ref, ref, mg_s.at[d, s - 1], mg_r.at[d, s - 1], ring[d])

    def md(i, core, rel, h):
        ref = mixer_piece(core, rel, h)
        return remote(ref, ref, md_s.at[i], md_r.at[i], partner)

    pieces = [(0, None)]
    for s in range(1, S):
        pieces += [(-s, None), (s, None)]
    pieces += [(S, 0), (S, 1)]

    mg(0, 1, False).start()
    mg(1, 1, False).start()
    md(0, k, *pieces[0]).start()

    @pl.when(active)
    def _():
        ret[pl.ds(pl.multiple_of(c * CAP, CAP), CAP), :] = fin[
            pl.ds(pl.multiple_of(half_c * CAP, CAP), CAP), :
        ]

    for s in range(1, S + 1):
        for d in range(2):
            mg(d, s, True).wait_recv()
            if s < S:
                mg(d, s + 1, False).start()
            i = 1 + (s - 1) * 2 + d
            md(i, k, *pieces[i]).start()

    def routed_piece(rel, h):
        return rout.at[pl.ds(h * (T // 2), T // 2), block(rel)]

    def rg(d, s, h, incoming):
        ref = routed_piece(-sign[d] * (s if incoming else s - 1), h)
        return remote(ref, ref, rg_s.at[d, s - 1, h], rg_r.at[d, s - 1, h], ring[d])

    rels = [0]
    for s in range(1, S):
        rels += [-s, s]
    rels += [S]

    def rd(i, h):
        ref = routed_piece(rels[i], h)
        return remote(ref, ref, rd_s.at[i, h], rd_r.at[i, h], partner)

    @pl.when(active)
    def _():
        def back(i, carry):
            e = (c + i) % E
            remote(
                fin.at[pl.ds(0, CAP), :],
                ret.at[pl.ds(pl.multiple_of(e * CAP, CAP), CAP), :],
                ret_s.at[0],
                ret_r.at[e],
                (c, t),
            ).wait_recv()
            return carry

        lax.fori_loop(1, E, back, 0)
        for h in range(2):
            rows = slice(h * (T // 2), (h + 1) * (T // 2))
            total = dot(whi[rows, :], ret[...]) + dot(wlo[rows, :], ret[...])
            rout[rows, cols_y] = total.astype(BF)
            for d in range(2):
                rg(d, 1, h, False).start()
            rd(0, h).start()
        for s in range(1, S + 1):
            for h in range(2):
                for d in range(2):
                    if s == S and h != d:
                        continue
                    rg(d, s, h, True).wait_recv()
                    if s + 1 < S or (s + 1 == S and h == d):
                        rg(d, s + 1, h, False).start()
                    rd(1 + (s - 1) * 2 + (d if s < S else 0), h).start()

    for i, piece in enumerate(pieces):
        md(i, k, *piece).wait_send()
        md(i, 1 - k, *piece).wait_recv()
    for one in weights:
        one.wait_send()
    send_halo.wait_send()
    send_g.wait_send()
    for s in range(1, S + 1):
        for d in range(2):
            mg(d, s, False).wait_send()
            for h in range(2):
                if s < S or h == d:
                    ag(d, s, h).wait_send()
                if s > 1 or h == d:
                    rs(d, s, h).wait_send()

    def gave(i, carry):
        @pl.when(2 * i + k != c)
        def _():
            giving(i).wait_send()

        return carry

    lax.fori_loop(0, E // 2, gave, 0)

    @pl.when(active)
    def _():
        def sent(i, carry):
            dispatch((c + i) % E).wait_send()
            return carry

        lax.fori_loop(1, E, sent, 0)
        for s in range(1, S + 1):
            for h in range(2):
                for d in range(2):
                    if s < S or h == d:
                        rg(d, s, h, False).wait_send()
        for i in range(len(rels)):
            for h in range(2):
                rd(i, h).wait_send()

    @pl.when(jnp.logical_not(active))
    def _():
        for i in range(len(rels)):
            for h in range(2):
                rd(i, h).wait_recv()


def on_device(E, Y, mrows, mgain, win, wgi, wgo, taps, wmo, rrows, rgain, ids, rw, eg, eu, ed):
    M, D = mrows.shape
    T = rrows.shape[0]
    HC = win.shape[1]
    FW = eg.shape[2]
    CW = D // Y
    S = Y // 2
    CAP = 2 * T * ids.shape[1] // E
    R = E * CAP // 2
    R2 = R // 2
    MQ = M // 4
    VM = pl.BlockSpec(memory_space=pltpu.VMEM)
    HB = pl.BlockSpec(memory_space=pl.ANY)
    DS = pltpu.SemaphoreType.DMA
    n_pieces = 2 * S + 1
    return pl.pallas_call(
        functools.partial(kernel, E, Y, CAP),
        out_shape=(
            jax.ShapeDtypeStruct((M, D), BF),
            jax.ShapeDtypeStruct((T, D), BF),
        ),
        in_specs=[HB, VM, HB, HB, HB, VM, HB, HB, VM, VM, VM, HB, HB, HB],
        out_specs=(VM, VM),
        scratch_shapes=[
            pltpu.VMEM((M, D), BF),
            pltpu.VMEM((M, D), BF),
            pltpu.VMEM((D, HC), BF),
            pltpu.VMEM((D, HC), BF),
            pltpu.VMEM((D, HC), BF),
            pltpu.VMEM((2 * HC, D), BF),
            pltpu.VMEM((T, D), BF),
            pltpu.VMEM((T, CW), BF),
            pltpu.VMEM((D, 4 * FW), BF),
            pltpu.VMEM((2 * FW, D), BF),
            pltpu.VMEM((2, T, 128), F32),
            pltpu.VMEM((E * CAP, CW), BF),
            pltpu.VMEM((Y, R, CW), BF),
            pltpu.VMEM((2, R2, 4 * FW), F32),
            pltpu.VMEM((2, R2, 2 * FW), BF),
            pltpu.VMEM((2, S, 2, R2 + MQ, CW), BF),
            pltpu.VMEM((2, S, 2, R2 + MQ, CW), BF),
            pltpu.VMEM((R, CW), BF),
            pltpu.VMEM((E * CAP, CW), BF),
            pltpu.VMEM((T, E * CAP), BF),
            pltpu.VMEM((T, E * CAP), BF),
            pltpu.VMEM((M, 128), BF),
            pltpu.VMEM((16, 128), BF),
            pltpu.VMEM((M + 16, 128), F32),
            pltpu.VMEM((M, 128), F32),
            pltpu.VMEM((M, 128), BF),
            pltpu.VMEM((M // 2, 128), BF),
            DS((9,)),
            DS((4,)),
            DS((4,)),
            DS((E,)),
            DS((E // 2,)),
            DS,
            DS,
            DS,
            DS,
            DS((2, S, 2)),
            DS((2, S, 2)),
            DS((2, S, 2)),
            DS((2, S, 2)),
            DS((E // 2,)),
            DS((E,)),
            DS((2, S)),
            DS((2, S)),
            DS((n_pieces,)),
            DS((n_pieces,)),
            DS((2, S, 2)),
            DS((2, S, 2)),
            DS((2 * S, 2)),
            DS((2 * S, 2)),
        ],
        compiler_params=pltpu.CompilerParams(collective_id=0, has_side_effects=True),
    )(
        mrows,
        mgain.reshape(1, D),
        win,
        wgi,
        wgo,
        taps,
        wmo,
        rrows,
        rgain.reshape(1, D),
        ids,
        rw,
        eg,
        eu,
        ed,
    )


def solution(mesh):
    E = mesh.shape["ep"]
    Y = mesh.shape["tp"] // 2
    return jax.shard_map(
        functools.partial(on_device, E, Y),
        mesh=mesh,
        in_specs=(
            P("ep", None),
            P(),
            P(None, "tp"),
            P(None, "tp"),
            P(None, "tp"),
            P(None, "tp"),
            P("tp", None),
            P("ep", None),
            P(),
            P("ep", None),
            P("ep", None),
            P("ep", None, "tp"),
            P("ep", None, "tp"),
            P("ep", "tp", None),
        ),
        out_specs=(P("ep", None), P("ep", None)),
        check_vma=False,
    )
```

time: 322 us -> 118 us (0.37)
  waiting for transfers between devices: 223 us -> 0 us
  Pallas kernels: 0 us -> 107 us
  blocking collectives: 24.8 us -> 0 us
  other arithmetic: 16.3 us -> 0 us
  matrix products: 13.6 us -> 0 us
  between operations: 14.1 us -> 0.67 us
  starting transfers between devices: 12.5 us -> 0 us
  local copies, waits for them, and re-layouts: 16.8 us -> 8.9 us
    psum x1 -> x0, waiting for transfers between devices: 117 us -> none  [packed_total(): so_far = lax.psum(jnp.concatenate([a.ravel() for a in arrays]), axis)]
    pallas_call x0 -> x1, Pallas kernels: none -> 107 us  [on_device(): pl.pallas_call(functools.partial(kernel, E, Y, CAP), out_shape=(jax.Shape...]
    reduce_scatter x1 -> x0, waiting for transfers between devices: 56.6 us -> none  [on_device(): lax.psum_scatter(jnp.dot(hidden, expert_down[0], preferred_element_type=j...]
    all_gather x1 -> x0, waiting for transfers between devices: 42.1 us -> none  [on_device(): incoming = lax.all_gather(arrived, 'tp', axis=0, tiled=True)]
    all_to_all x1 -> x0, blocking collectives: 24.8 us -> none  [on_device(): lax.all_to_all(outgoing, 'ep', split_axis=1, concat_axis=1, tiled=True)]
    dot_general x5 -> x0, matrix products: 13.6 us -> none  [the longest x1 8.47 us: on_device(): jnp.dot(hidden, expert_down[0], preferred_element_type=jnp.float32)]
    reduce_sum x5 -> x0, other arithmetic: 12 us -> none  [the longest x1 9.87 us: on_device(): jnp.sum(contrib.reshape(tok_count, pick_count, model_width), axis=1)]
    all_to_all x1 -> x0, starting transfers between devices: 9.09 us -> none  [on_device(): lax.all_to_all(summed.reshape(share_rows, experts, model_width), 'ep', sp...]
  transfers between devices with their start and end apart: 5 -> 0, of which waited for: 4 -> 0; matrix products, arithmetic and copies ran while one was open for 2% -> 0% of each run, Pallas kernels for 0% -> 0%
where the time goes in v1:
time: 118 us; the launch traced here: 117 us
  Pallas kernels  107 us (91%)
  local copies, waits for them, and re-layouts  8.9 us (8%)
    pallas_call x1, Pallas kernels, on_device(): pl.pallas_call(functools.partial(kernel, E, Y, CAP), out_shape=(jax.Shape...  107 us
    unnamed x17, local copies, waits for them, and re-layouts  8.9 us

profile of v1, /device:TPU:1, one launch (start us, length us, event | category | flops | bytes accessed | tf_op | source)
XLA Modules:
  0.0 117.0 jit_solution(16950271056468650316)
XLA Ops:
  0.6 0.0 copy-start.4
  0.6 0.0 copy-start.1
  0.6 0.7 copy-done.4
  1.3 0.8 copy.19.ids_ref
  2.1 1.5 %copy.20.rw_ref = f32[256,2]{1,0:T(8,128)} copy(f32[256,2]{0,1:T(2,128)} %param.24) | data formatting | bytes 4096 | tf_op args[10]
  3.6 0.0 copy-done.1
  3.6 0.0 copy-start.2
  3.6 1.0 copy.16.win_hbm
  4.6 0.0 copy-done.2
  4.6 0.0 copy-start.3
  4.6 1.0 copy.17.wgi_hbm
  5.6 0.0 copy-done.3
  5.6 1.0 copy.18.wgo_hbm
  6.6 107.4 %shard_map.149 = (bf16[128,2048]{1,0:T(8,128)(2,1)}, bf16[256,2048]{1,0:T(8,128)(2,1)}) custom-call(bf16[128,2048]{1,0:T(8,128)(2,1)} %mrows_hbm.1, f32[1,2048]{1,0:T(1,128)} %bitcast.2, bf16[2048,64]{1,0:T(8,128)(2,1)} %copy.16.win_hbm, bf16[2048,64]{1,0:T(8,128)(2,1)} %copy.17.wgi_hbm, bf16[2048,64]{1,0:T(8,128)(2,1)} %copy.18.wgo_hbm, f32[3,64]{1,0:T(4,128)} %taps.1, ...), custom_call_target="tpu_custom_call" | custom-call | tf_op jit(solution)/shard_map/pallas_call | solution.py:535
  114.1 0.0 copy-start
  114.1 2.0 %copy.23 = bf16[128,2048]{1,0:T(8,128)(2,1)} copy(bf16[128,2048]{1,0:T(8,128)(2,1)} %get-tuple-element.4) | data formatting | bytes 1048576
  116.0 0.0 copy-done
  116.0 1.0 copy.24
Async XLA Ops:
  0.6 0.7 copy-start.4
  0.6 2.9 %copy-start.1 = (bf16[2048,64]{0,1:T(8,128)(2,1)S(1)}, bf16[2048,64]{0,1:T(8,128)(2,1)}, u32[]{:S(2)}) copy-start(bf16[2048,64]{0,1:T(8,128)(2,1)} %param.16) | copy-start | bytes 786436
  3.6 1.0 copy-start.2
  4.6 1.0 copy-start.3
  114.1 2.0 %copy-start = (bf16[256,2048]{1,0:T(8,128)(2,1)S(1)}, bf16[256,2048]{1,0:T(8,128)(2,1)}, u32[]{:S(2)}) copy-start(bf16[256,2048]{1,0:T(8,128)(2,1)} %get-tuple-element.5) | copy-start | bytes 3145732

commit v2 on v1

v2 whole, which is shorter than its diff:
```python
import functools

import jax
import jax.numpy as jnp
from jax import lax
from jax.experimental import pallas as pl
from jax.experimental.pallas import tpu as pltpu
from jax.sharding import PartitionSpec as P

MESH = pl.DeviceIdType.MESH
BF = jnp.bfloat16
F32 = jnp.float32
EPS = 1e-06


def dot(a, b):
    return jnp.dot(a, b, preferred_element_type=F32)


def dot_t(a, b):
    return lax.dot_general(a, b, (((1,), (1,)), ((), ())), preferred_element_type=F32)


def kernel(
    E,
    Y,
    X,
    NW,
    CAP,
    mrows_hbm,
    mgain_hbm,
    win_hbm,
    wgi_hbm,
    wgo_hbm,
    taps_hbm,
    wmo_hbm,
    rrows_hbm,
    rgain_hbm,
    ids_hbm,
    rw_hbm,
    eg_hbm,
    eu_hbm,
    ed_hbm,
    mout,
    rout,
    mgain,
    taps,
    rgain,
    ids_ref,
    rw_ref,
    mrows,
    mn,
    win,
    wgi,
    wgo,
    wmo,
    rrows,
    nrm,
    nfull,
    rscale,
    wgu,
    wd,
    slots,
    slotrow,
    xs,
    xsn,
    xb,
    xn,
    acc,
    hid,
    sbuf,
    rbuf,
    fin,
    ret,
    whi,
    wlo,
    ci,
    halo,
    ext,
    go,
    gsc,
    gpart,
    l_sem,
    wt_s,
    wt_r,
    a2a_s,
    a2a_r,
    halo_s,
    halo_r,
    g_s,
    g_r,
    ag_s,
    ag_r,
    rs_s,
    rs_r,
    ret_s,
    ret_r,
    mg_s,
    mg_r,
    md_s,
    md_r,
    rg_s,
    rg_r,
    rd_s,
    rd_r,
):
    S = Y // 2
    c = lax.axis_index("ep")
    t = lax.axis_index("tp")
    y = t // 2
    k = t % 2
    half_c = c // 2
    z = c // X
    x = c % X
    active = k == c % 2
    M, D = mn.shape
    T = nrm.shape[0]
    CW = D // Y
    NS = E * CAP
    R = NS // 2
    R2 = R // 2
    Z = E // X
    NN = 2 * NW + 1
    NF = Z - NN
    PS = X * CAP
    NP = NN * X // 2
    FP = NF * X // 2
    RN = NP * CAP
    RF = FP * CAP
    RF2 = RF // 2
    MH = M // 2
    MQ = M // 4
    HC = win.shape[0]
    EP = -(-E // 16) * 16
    partner = (c, y * 2 + 1 - k)
    ring = [(c, ((y + 1) % Y) * 2 + k), (c, ((y + Y - 1) % Y) * 2 + k)]
    sign = [1, -1]

    def remote(src, dst, ss, rs, dev):
        return pltpu.make_async_remote_copy(
            src_ref=src, dst_ref=dst, send_sem=ss, recv_sem=rs, device_id=dev, device_id_type=MESH
        )

    barrier = pltpu.get_barrier_semaphore()

    def greet(i, carry):
        pl.semaphore_signal(barrier, inc=1, device_id=((c + i) % E, t), device_id_type=MESH)
        return carry

    for dev in (partner, ring[0], ring[1]):
        pl.semaphore_signal(barrier, inc=1, device_id=dev, device_id_type=MESH)
    lax.fori_loop(1, E, greet, 0)

    FW = eg_hbm.shape[2]
    loads = [
        pltpu.make_async_copy(rrows_hbm, rrows, l_sem.at[0]),
        pltpu.make_async_copy(mrows_hbm, mrows, l_sem.at[1]),
        pltpu.make_async_copy(win_hbm, win, l_sem.at[2]),
        pltpu.make_async_copy(wgi_hbm, wgi, l_sem.at[3]),
        pltpu.make_async_copy(wgo_hbm, wgo, l_sem.at[4]),
        pltpu.make_async_copy(eg_hbm.at[0], wgu.at[:, pl.ds(0, FW)], l_sem.at[5]),
        pltpu.make_async_copy(eu_hbm.at[0], wgu.at[:, pl.ds(2 * FW, FW)], l_sem.at[6]),
        pltpu.make_async_copy(ed_hbm.at[0], wd.at[pl.ds(0, FW), :], l_sem.at[7]),
        pltpu.make_async_copy(wmo_hbm, wmo.at[pl.ds(0, HC), :], l_sem.at[8]),
        pltpu.make_async_copy(ids_hbm, ids_ref, l_sem.at[9]),
        pltpu.make_async_copy(rw_hbm, rw_ref, l_sem.at[10]),
        pltpu.make_async_copy(rgain_hbm, rgain, l_sem.at[11]),
        pltpu.make_async_copy(mgain_hbm, mgain, l_sem.at[12]),
        pltpu.make_async_copy(taps_hbm, taps, l_sem.at[13]),
    ]
    for i in (9, 10, 0, 11, 1, 12, 2, 3, 4, 13, 5, 6, 7, 8):
        loads[i].start()

    def slot_numbers():
        ids = ids_ref[...]
        expert = lax.broadcasted_iota(jnp.int32, (EP, T), 0)
        hit0 = expert == ids[0:1, :]
        hit1 = expert == ids[1:2, :]
        named = jnp.where(hit0 | hit1, 1.0, 0.0).astype(BF)
        r = lax.broadcasted_iota(jnp.int32, (T, T), 0)
        q = lax.broadcasted_iota(jnp.int32, (T, T), 1)
        upper = jnp.where(r < q, 1.0, 0.0).astype(BF)
        before = dot(named, upper)
        row0 = ids[0:1, :].astype(F32) * CAP + jnp.sum(
            jnp.where(hit0, before, 0.0), axis=0, keepdims=True
        )
        row1 = ids[1:2, :].astype(F32) * CAP + jnp.sum(
            jnp.where(hit1, before, 0.0), axis=0, keepdims=True
        )
        diag = r == q

        def column(row):
            one = jnp.sum(jnp.where(diag, row, 0.0), axis=1, keepdims=True)
            return jnp.broadcast_to(one, (T, 128))

        columns = (row0, row1, rw_ref[0:1, :], rw_ref[1:2, :])
        for i, row in enumerate(columns):
            slots[i] = column(row)
        return row0, row1

    cols_y = pl.ds(pl.multiple_of(y * CW, CW), CW)

    def norm_routed():
        step = 32

        def body(i, carry):
            rows = pl.ds(pl.multiple_of(i * step, step), step)
            v = rrows[rows, :].astype(F32)
            scale = lax.rsqrt(jnp.mean(v * v, axis=-1, keepdims=True) + EPS)
            rscale[rows, :] = jnp.broadcast_to(scale, (step, 128))
            part = rrows[rows, cols_y].astype(F32)
            nrm[rows, :] = (part * scale * rgain[:, cols_y]).astype(BF)
            return carry

        lax.fori_loop(0, T // step, body, 0)

    loads[9].wait()
    loads[10].wait()

    CH = NS // 4

    def place(zc, xc, ze):
        return (zc - ze + Z + NW) % Z * (X // 2) + xc // 2

    def cap_rows(i):
        return pl.ds(pl.multiple_of(i * CAP, CAP), CAP)

    def far(i):
        q = i % NF
        ze = (z + NW + 1 + q) % Z
        xe = (x + i // NF) % X
        p = place(z, x, ze)
        return remote(
            xs.at[cap_rows(q * X + xe), :],
            xb.at[y, cap_rows(p - NP), :],
            a2a_s.at[q * X + xe],
            a2a_r.at[p],
            (ze * X + xe, t),
        )

    def near(i):
        n = i % NN
        ze = (z + Z - NW + n) % Z
        xe = (x + i // NN) % X
        p = place(z, x, ze)
        return remote(
            xsn.at[cap_rows(n * X + xe), :],
            xn.at[cap_rows(p), :],
            a2a_s.at[NF * X + n * X + xe],
            a2a_r.at[p],
            (ze * X + xe, t),
        )

    def pick_plane(zp):
        number = lax.broadcasted_iota(jnp.int32, (PS, T), 0) + zp * PS
        row0 = slotrow[0:1, :].astype(jnp.int32)
        row1 = slotrow[1:2, :].astype(jnp.int32)
        return jnp.where((number == row0) | (number == row1), 1.0, 0.0).astype(BF)

    def plane_rows(q):
        return pl.ds(pl.multiple_of(q * PS, PS), PS)

    @pl.when(active)
    def _():
        row0, row1 = slot_numbers()
        loads[0].wait()
        loads[11].wait()
        norm_routed()
        slotrow[0:1, :] = row0
        slotrow[1:2, :] = row1

        def select(q, carry):
            pick = pick_plane((z + NW + 1 + q) % Z)
            xs[plane_rows(q), :] = dot(pick, nrm[...]).astype(BF)
            return carry

        lax.fori_loop(0, NF, select, 0)

    @pl.when(jnp.logical_not(active))
    def _():
        loads[0].wait()
        loads[11].wait()

    pl.semaphore_wait(barrier, E + 2)

    @pl.when(active)
    def _():
        def send_far(i, carry):
            far(i).start()
            return carry

        lax.fori_loop(0, NF * X, send_far, 0)

        def norm_full(i, carry):
            rows = pl.ds(pl.multiple_of(i * 16, 16), 16)
            v = rrows[rows, :].astype(F32)
            nfull[rows, :] = (v * rscale[rows, 0:1] * rgain[...]).astype(BF)
            return carry

        lax.fori_loop(0, T // 16, norm_full, 0)

        def select_near(n, carry):
            pick = pick_plane((z + Z - NW + n) % Z)
            xsn[plane_rows(n), :] = dot(pick, nfull[...]).astype(BF)
            return carry

        lax.fori_loop(0, NN, select_near, 0)

        def send_near(i, carry):
            @pl.when(i != NW)
            def _():
                near(i).start()

            return carry

        lax.fori_loop(0, NN * X, send_near, 0)
        xn[cap_rows(place(z, x, z)), :] = xsn[cap_rows(NW * X + x), :]

    weights = [
        remote(eg_hbm.at[0], wgu.at[:, pl.ds(FW, FW)], wt_s.at[0], wt_r.at[0], partner),
        remote(eu_hbm.at[0], wgu.at[:, pl.ds(3 * FW, FW)], wt_s.at[1], wt_r.at[1], partner),
        remote(ed_hbm.at[0], wd.at[pl.ds(FW, FW), :], wt_s.at[2], wt_r.at[2], partner),
        remote(wmo_hbm, wmo.at[pl.ds(HC, HC), :], wt_s.at[3], wt_r.at[3], partner),
    ]
    for one in weights:
        one.start()

    for i in (1, 2, 3, 4, 12, 13):
        loads[i].wait()

    def norm_mixer(i, carry):
        rows = pl.ds(pl.multiple_of(i * 16, 16), 16)
        v = mrows[rows, :].astype(F32)
        scale = lax.rsqrt(jnp.mean(v * v, axis=-1, keepdims=True) + EPS)
        mn[rows, :] = (v * scale * mgain[...]).astype(BF)
        return carry

    lax.fori_loop(0, M // 16, norm_mixer, 0)
    normed = mn[...]
    inner = dot_t(normed, win[...])
    gate_in = dot_t(normed, wgi[...])
    go[:, 0:HC] = dot_t(normed, wgo[...])
    ci[...] = jnp.zeros(ci.shape, BF)
    ci[:, 0:HC] = (gate_in * inner).astype(BF)
    send_halo = remote(ci.at[pl.ds(M - 16, 16), :], halo, halo_s, halo_r, ((c + 1) % E, t))
    send_halo.start()

    @pl.when(active)
    def _():
        for i in range(4):
            number = lax.broadcasted_iota(jnp.int32, (T, CH), 1) + i * CH
            s0 = slots[0][:, 0:1].astype(jnp.int32)
            s1 = slots[1][:, 0:1].astype(jnp.int32)
            w = jnp.where(number == s0, slots[2][:, 0:1], 0.0) + jnp.where(
                number == s1, slots[3][:, 0:1], 0.0
            )
            top = w.astype(BF)
            whi[:, i * CH : (i + 1) * CH] = top
            wlo[:, i * CH : (i + 1) * CH] = (w - top.astype(F32)).astype(BF)

    def ag(d, s, h):
        blk = (y + Y - sign[d] * (s - 1)) % Y
        ref = xb.at[blk, pl.ds(h * RF2, RF2), :]
        return remote(ref, ref, ag_s.at[d, s - 1, h], ag_r.at[d, s - 1, h], ring[d])

    def ag_wait(d, s, h):
        blk = (y + Y - sign[d] * s) % Y
        ref = xb.at[blk, pl.ds(h * RF2, RF2), :]
        remote(ref, ref, ag_s.at[d, s - 1, h], ag_r.at[d, s - 1, h], ring[d]).wait_recv()

    def gate_up(blk, h):
        return dot(
            xb[blk, h * RF2 : (h + 1) * RF2, :], wgu[pl.ds(pl.multiple_of(blk * CW, CW), CW), :]
        )

    def far_arrived(i, carry):
        remote(
            xs.at[pl.ds(0, CAP), :],
            xb.at[y, cap_rows(i), :],
            a2a_s.at[0],
            a2a_r.at[NP + i],
            (c, t),
        ).wait_recv()
        return carry

    def near_arrived(i, carry):
        @pl.when(jnp.logical_not(active & (i == place(z, x, z))))
        def _():
            remote(
                xsn.at[pl.ds(0, CAP), :], xn.at[cap_rows(i), :], a2a_s.at[0], a2a_r.at[i], (c, t)
            ).wait_recv()

        return carry

    def finish(both, rows):
        g = both[:, 0 : 2 * FW]
        hid[rows, :] = (g / (1.0 + jnp.exp(-g)) * both[:, 2 * FW :]).astype(BF)

    for s in range(1, S + 2):
        for h in range(2):
            if s == 1:
                lax.fori_loop(h * (FP // 2), (h + 1) * (FP // 2), far_arrived, 0)
            for d in range(2):
                if s > 1 and (s - 1 < S or h == d):
                    ag_wait(d, s - 1, h)
                if s <= S and (s < S or h == d):
                    ag(d, s, h).start()
            if s == 1 and h == 0:
                loads[5].wait()
                loads[6].wait()
                weights[0].wait_recv()
                weights[1].wait_recv()
            if s == 1:
                acc[h] = gate_up(y, h)
            elif s <= S:
                acc[h] += gate_up((y + s - 1) % Y, h) + gate_up((y + Y - s + 1) % Y, h)
            else:
                finish(
                    acc[h] + gate_up((y + S) % Y, h), slice(RN + h * RF2, RN + (h + 1) * RF2)
                )
        if s == S:
            lax.fori_loop(0, NP, near_arrived, 0)
            finish(dot(xn[...], wgu[...]), slice(0, RN))
        if s == 2:
            send_halo.wait_recv()
            ext[0:16, :] = jnp.where(c > 0, halo[...].astype(F32), 0.0)
            ext[16:, :] = ci[...].astype(F32)
            conv = taps[0:1, :] * ext[14 : 14 + M, 0:HC]
            conv = conv + taps[1:2, :] * ext[15 : 15 + M, 0:HC]
            conv = conv + taps[2:3, :] * ext[16 : 16 + M, 0:HC]
            gsc[...] = jnp.zeros(gsc.shape, BF)
            gsc[:, 0:HC] = (go[:, 0:HC] * conv).astype(BF)
            send_g = remote(
                gsc.at[pl.ds(pl.multiple_of((1 - k) * MH, MH), MH), :], gpart, g_s, g_r, partner
            )
            send_g.start()

    loads[7].wait()
    loads[8].wait()
    weights[2].wait_recv()
    weights[3].wait_recv()
    send_g.wait_recv()

    def partial(h, dest):
        cols = pl.ds(pl.multiple_of(dest * CW, CW), CW)
        mine = gsc[pl.ds(pl.multiple_of(k * MH + h * MQ, MQ), MQ), :]
        other = gpart[h * MQ : (h + 1) * MQ, :]
        return dot(hid[h * R2 : (h + 1) * R2, :], wd[:, cols]), dot(mine[:, 0:HC], wmo[0:HC, cols]) + dot(
            other[:, 0:HC], wmo[HC:, cols]
        )

    def rs(d, s, h):
        return remote(
            sbuf.at[d, s - 1, h], rbuf.at[d, s - 1, h], rs_s.at[d, s - 1, h], rs_r.at[d, s - 1, h], ring[d]
        )

    order = [(1, 0, 0), (1, 1, 1)]
    for s in range(2, S + 1):
        order += [(s, 1, 0), (s, 0, 1), (s, 0, 0), (s, 1, 1)]
    for s, h, d in order:
        a, b = partial(h, (y + Y + sign[d] * (S + 1 - s)) % Y)
        if s > 2 or (s == 2 and h == d):
            rs(d, s - 1, h).wait_recv()
            a = a + rbuf[d, s - 2, h, 0:R2, :].astype(F32)
            b = b + rbuf[d, s - 2, h, R2:, :].astype(F32)
        sbuf[d, s - 1, h, 0:R2, :] = a.astype(BF)
        sbuf[d, s - 1, h, R2:, :] = b.astype(BF)
        rs(d, s, h).start()

    def target(i):
        zc = (z + Z - NW + i // (X // 2)) % Z
        return zc * X + i % (X // 2) * 2 + k

    def giving(i):
        return remote(
            fin.at[cap_rows(i), :], ret.at[cap_rows(c), :], ret_s.at[i], ret_r.at[c], (target(i), t)
        )

    def give(i, carry):
        @pl.when(target(i) != c)
        def _():
            giving(i).start()

        return carry

    for h in range(2):
        a, b = partial(h, y)
        for d in (1 - h, h):
            rs(d, S, h).wait_recv()
            a = a + rbuf[d, S - 1, h, 0:R2, :].astype(F32)
            b = b + rbuf[d, S - 1, h, R2:, :].astype(F32)
        fin[h * R2 : (h + 1) * R2, :] = a.astype(BF)
        mout[pl.ds(pl.multiple_of(k * MH + h * MQ, MQ), MQ), cols_y] = b.astype(BF)
        lax.fori_loop(h * (E // 4), (h + 1) * (E // 4), give, 0)

    def block(rel):
        return pl.ds(pl.multiple_of(((y + Y + rel) % Y) * CW, CW), CW)

    def mixer_piece(core, rel):
        return mout.at[pl.ds(pl.multiple_of(core * MH, MH), MH), block(rel)]

    def mg(i, rel):
        ref = mixer_piece(k, rel)
        return remote(ref, ref, mg_s.at[i], mg_r.at[i], (c, ((y + i) % Y) * 2 + k))

    def md(i, core):
        ref = mixer_piece(core, -i)
        return remote(ref, ref, md_s.at[i], md_r.at[i], partner)

    for i in range(1, S):
        mg(i, 0).start()
        mg(Y - i, 0).start()
    mg(S, 0).start()
    md(0, k).start()

    @pl.when(active)
    def _():
        ret[cap_rows(c), :] = fin[cap_rows(place(z, x, z)), :]

    def pass_mixer():
        for i in range(1, Y):
            mg(i, -i).wait_recv()
            md(i, k).start()

    def routed_piece(rel, h):
        return rout.at[pl.ds(h * (T // 2), T // 2), block(rel)]

    def pieces(j):
        return [(d, h) for h in range(2) for d in range(2) if j < S or h == d]

    def rg(d, j, h, incoming):
        if incoming:
            ref = routed_piece(-sign[d] * j, h)
        else:
            ref = routed_piece(0 if j <= 2 else -sign[d] * 2, h)
        dev = (c, ((y + Y + sign[d] * (j if j <= 2 else j - 2)) % Y) * 2 + k)
        return remote(ref, ref, rg_s.at[d, j - 1, h], rg_r.at[d, j - 1, h], dev)

    def rd(d, j, h):
        i = 0 if j == 0 else 1 + (j - 1) * 2 + (d if j < S else 0)
        ref = routed_piece(-sign[d] * j, h)
        return remote(ref, ref, rd_s.at[i, h], rd_r.at[i, h], partner)

    shared = [(0, 0, 0), (0, 0, 1)]
    for j in range(1, S + 1):
        shared += [(d, j, h) for d, h in pieces(j)]

    @pl.when(active)
    def _():
        def back(i, carry):
            e = (c + i) % E
            remote(
                fin.at[pl.ds(0, CAP), :],
                ret.at[pl.ds(pl.multiple_of(e * CAP, CAP), CAP), :],
                ret_s.at[0],
                ret_r.at[e],
                (c, t),
            ).wait_recv()
            return carry

        lax.fori_loop(1, E, back, 0)
        for h in range(2):
            rows = slice(h * (T // 2), (h + 1) * (T // 2))
            total = dot(whi[rows, :], ret[...]) + dot(wlo[rows, :], ret[...])
            rout[rows, cols_y] = total.astype(BF)
            for d in range(2):
                if 2 < S or h == d:
                    rg(d, 2, h, False).start()
            rd(0, 0, h).start()
        for d, h in pieces(1):
            rg(d, 1, h, False).start()
        pass_mixer()
        for d, h in pieces(2):
            rg(d, 2, h, True).wait_recv()
            for j in range(S, 2, -1):
                if (d, h) in pieces(j):
                    rg(d, j, h, False).start()
            rd(d, 2, h).start()
        for j in [1] + list(range(3, S + 1)):
            for d, h in pieces(j):
                rg(d, j, h, True).wait_recv()
                rd(d, j, h).start()

    @pl.when(jnp.logical_not(active))
    def _():
        pass_mixer()

    for i in range(Y):
        md(i, k).wait_send()
        md(i, 1 - k).wait_recv()
        if i > 0:
            mg(i, 0).wait_send()
    for one in weights:
        one.wait_send()
    send_halo.wait_send()
    send_g.wait_send()
    for s in range(1, S + 1):
        for d in range(2):
            for h in range(2):
                if s < S or h == d:
                    ag(d, s, h).wait_send()
                if s > 1 or h == d:
                    rs(d, s, h).wait_send()

    def gave(i, carry):
        @pl.when(target(i) != c)
        def _():
            giving(i).wait_send()

        return carry

    lax.fori_loop(0, E // 2, gave, 0)

    @pl.when(active)
    def _():
        def sent_far(i, carry):
            far(i).wait_send()
            return carry

        def sent_near(i, carry):
            @pl.when(i != NW)
            def _():
                near(i).wait_send()

            return carry

        lax.fori_loop(0, NF * X, sent_far, 0)
        lax.fori_loop(0, NN * X, sent_near, 0)
        for j in range(1, S + 1):
            for d, h in pieces(j):
                rg(d, j, h, False).wait_send()
        for one in shared:
            rd(*one).wait_send()

    @pl.when(jnp.logical_not(active))
    def _():
        for one in shared:
            rd(*one).wait_recv()


def on_device(E, Y, mrows, mgain, win, wgi, wgo, taps, wmo, rrows, rgain, ids, rw, eg, eu, ed):
    M, D = mrows.shape
    T = rrows.shape[0]
    HC = win.shape[1]
    FW = eg.shape[2]
    CW = D // Y
    S = Y // 2
    CAP = 2 * T * ids.shape[1] // E
    X = 4
    NW = 1 if E // X > 3 else 0
    RN = (2 * NW + 1) * (X // 2) * CAP
    R = E * CAP // 2
    R2 = R // 2
    MQ = M // 4
    VM = pl.BlockSpec(memory_space=pltpu.VMEM)
    HB = pl.BlockSpec(memory_space=pl.ANY)
    DS = pltpu.SemaphoreType.DMA
    return pl.pallas_call(
        functools.partial(kernel, E, Y, X, NW, CAP),
        out_shape=(pltpu.VMEM((M, D), BF), pltpu.VMEM((T, D), BF)),
        in_specs=[HB] * 14,
        out_specs=(VM, VM),
        scratch_shapes=[
            pltpu.VMEM((1, D), F32),
            pltpu.VMEM(taps.shape, F32),
            pltpu.VMEM((1, D), F32),
            pltpu.VMEM((2, T), jnp.int32),
            pltpu.VMEM((2, T), F32),
            pltpu.VMEM((M, D), BF),
            pltpu.VMEM((M, D), BF),
            pltpu.VMEM((HC, D), BF),
            pltpu.VMEM((HC, D), BF),
            pltpu.VMEM((HC, D), BF),
            pltpu.VMEM((2 * HC, D), BF),
            pltpu.VMEM((T, D), BF),
            pltpu.VMEM((T, CW), BF),
            pltpu.VMEM((T, D), BF),
            pltpu.VMEM((T, 128), F32),
            pltpu.VMEM((D, 4 * FW), BF),
            pltpu.VMEM((2 * FW, D), BF),
            pltpu.VMEM((4, T, 128), F32),
            pltpu.VMEM((8, T), F32),
            pltpu.VMEM(((R - RN) * 2, CW), BF),
            pltpu.VMEM((2 * RN, D), BF),
            pltpu.VMEM((Y, R - RN, CW), BF),
            pltpu.VMEM((RN, D), BF),
            pltpu.VMEM((2, (R - RN) // 2, 4 * FW), F32),
            pltpu.VMEM((R, 2 * FW), BF),
            pltpu.VMEM((2, S, 2, R2 + MQ, CW), BF),
            pltpu.VMEM((2, S, 2, R2 + MQ, CW), BF),
            pltpu.VMEM((R, CW), BF),
            pltpu.VMEM((E * CAP, CW), BF),
            pltpu.VMEM((T, E * CAP), BF),
            pltpu.VMEM((T, E * CAP), BF),
            pltpu.VMEM((M, 128), BF),
            pltpu.VMEM((16, 128), BF),
            pltpu.VMEM((M + 16, 128), F32),
            pltpu.VMEM((M, 128), F32),
            pltpu.VMEM((M, 128), BF),
            pltpu.VMEM((M // 2, 128), BF),
            DS((14,)),
            DS((4,)),
            DS((4,)),
            DS((E,)),
            DS((E // 2,)),
            DS,
            DS,
            DS,
            DS,
            DS((2, S, 2)),
            DS((2, S, 2)),
            DS((2, S, 2)),
            DS((2, S, 2)),
            DS((E // 2,)),
            DS((E,)),
            DS((Y,)),
            DS((Y,)),
            DS((Y,)),
            DS((Y,)),
            DS((2, S, 2)),
            DS((2, S, 2)),
            DS((2 * S, 2)),
            DS((2 * S, 2)),
        ],
        compiler_params=pltpu.CompilerParams(collective_id=0, has_side_effects=True),
    )(
        mrows,
        mgain.reshape(1, D),
        win.T,
        wgi.T,
        wgo.T,
        taps,
        wmo,
        rrows,
        rgain.reshape(1, D),
        ids.T,
        rw.T,
        eg,
        eu,
        ed,
    )


def solution(mesh):
    E = mesh.shape["ep"]
    Y = mesh.shape["tp"] // 2
    return jax.shard_map(
        functools.partial(on_device, E, Y),
        mesh=mesh,
        in_specs=(
            P("ep", None),
            P(),
            P(None, "tp"),
            P(None, "tp"),
            P(None, "tp"),
            P(None, "tp"),
            P("tp", None),
            P("ep", None),
            P(),
            P("ep", None),
            P("ep", None),
            P("ep", None, "tp"),
            P("ep", None, "tp"),
            P("ep", "tp", None),
        ),
        out_specs=(P("ep", None), P("ep", None)),
        check_vma=False,
    )
```

time: 118 us -> 95.8 us (0.81)
  Pallas kernels: 107 us -> 93.2 us
  local copies, waits for them, and re-layouts: 8.9 us -> 1.77 us
    pallas_call x1, Pallas kernels: 107 us -> 93.2 us  [on_device(): pl.pallas_call(functools.partial(kernel, E, Y, X, NW, CAP), out_shape=(pl...]
    unnamed x17 -> x2, local copies, waits for them, and re-layouts: 8.9 us -> 1.77 us
where the time goes in v2:
time: 95.8 us; the launch traced here: 95.6 us
  Pallas kernels  93.2 us (97%)
  local copies, waits for them, and re-layouts  1.77 us (2%)
    pallas_call x1, Pallas kernels, on_device(): pl.pallas_call(functools.partial(kernel, E, Y, X, NW, CAP), out_shape=(pl...  93.2 us

profile of v2, /device:TPU:1, one launch (start us, length us, event | category | flops | bytes accessed | tf_op | source)
XLA Modules:
  0.0 95.6 jit_solution(10392288388588902634)
XLA Ops:
  0.6 93.2 %shard_map.149 = (bf16[128,2048]{1,0:T(8,128)(2,1)S(1)}, bf16[256,2048]{1,0:T(8,128)(2,1)S(1)}) custom-call(bf16[128,2048]{1,0:T(8,128)(2,1)} %mrows_hbm.1, f32[1,2048]{1,0:T(1,128)} %bitcast.10, bf16[64,2048]{1,0:T(8,128)(2,1)} %bitcast.7, bf16[64,2048]{1,0:T(8,128)(2,1)} %bitcast.8, bf16[64,2048]{1,0:T(8,128)(2,1)} %bitcast.9, f32[3,64]{1,0:T(4,128)} %taps_hbm.1, ...), custom_call_target="tpu_custom_call" | custom-call | tf_op jit(solution)/shard_map/pallas_call | solution.py:658
  93.9 0.8 copy.18
  94.7 1.0 %copy.19 = bf16[256,2048]{1,0:T(8,128)(2,1)} copy(bf16[256,2048]{1,0:T(8,128)(2,1)S(1)} %get-tuple-element.3) | data formatting | bytes 2097152

commit v3 on v2

v3 whole, which is shorter than its diff:
```python
import functools

import jax
import jax.numpy as jnp
from jax import lax
from jax.experimental import pallas as pl
from jax.experimental.pallas import tpu as pltpu
from jax.sharding import PartitionSpec as P

MESH = pl.DeviceIdType.MESH
BF = jnp.bfloat16
F32 = jnp.float32
EPS = 1e-06


def dot(a, b):
    return jnp.dot(a, b, preferred_element_type=F32)


def dot_t(a, b):
    return lax.dot_general(a, b, (((1,), (1,)), ((), ())), preferred_element_type=F32)


def kernel(
    E,
    Y,
    X,
    NW,
    CAP,
    mrows_hbm,
    mgain_hbm,
    win_hbm,
    wgi_hbm,
    wgo_hbm,
    taps_hbm,
    wmo_hbm,
    rrows_hbm,
    rgain_hbm,
    ids_hbm,
    rw_hbm,
    eg_hbm,
    eu_hbm,
    ed_hbm,
    mout,
    rout,
    mgain,
    taps,
    rgain,
    ids_ref,
    rw_ref,
    mrows,
    mn,
    win,
    wgi,
    wgo,
    wmo,
    rrows,
    nrm,
    nfull,
    rscale,
    wgu,
    wd,
    slotrow,
    xs,
    xsn,
    xb,
    xn,
    acc,
    hid,
    sbuf,
    rbuf,
    msbuf,
    mrbuf,
    fin,
    ret,
    whi,
    wlo,
    ci,
    halo,
    ext,
    go,
    gsc,
    gpart,
    l_sem,
    wt_s,
    wt_r,
    a2a_s,
    a2a_r,
    halo_s,
    halo_r,
    g_s,
    g_r,
    ag_s,
    ag_r,
    rs_s,
    rs_r,
    mx_s,
    mx_r,
    ret_s,
    ret_r,
    mg_s,
    mg_r,
    md_s,
    md_r,
    rg_s,
    rd_s,
    rd_r,
):
    S = Y // 2
    c = lax.axis_index("ep")
    t = lax.axis_index("tp")
    y = t // 2
    k = t % 2
    z = c // X
    x = c % X
    active = k == c % 2
    M, D = mn.shape
    T = nrm.shape[0]
    CW = D // Y
    NS = E * CAP
    R = NS // 2
    Z = E // X
    NN = 2 * NW + 1
    NF = Z - NN
    PS = X * CAP
    NP = NN * X // 2
    FP = NF * X // 2
    RN = NP * CAP
    RF = FP * CAP
    QS = PS // 2
    near_off = list(range(-NW, NW + 1))
    far_off = sorted(range(NW + 1, Z - NW), key=lambda g: min(g, Z - g))
    order_off = far_off + near_off
    RH = R // 2
    CH = CW // 2
    MH = M // 2
    MQ = MH // 2
    HC = win.shape[0]
    EP = -(-E // 16) * 16
    partner = (c, y * 2 + 1 - k)
    ring = [(c, ((y + 1) % Y) * 2 + k), (c, ((y + Y - 1) % Y) * 2 + k)]
    sign = [1, -1]

    def remote(src, dst, ss, rs, dev):
        return pltpu.make_async_remote_copy(
            src_ref=src, dst_ref=dst, send_sem=ss, recv_sem=rs, device_id=dev, device_id_type=MESH
        )

    def settle(ref, sem):
        pltpu.make_async_copy(ref, ref, sem).wait()

    FW = eg_hbm.shape[2]
    loads = [
        pltpu.make_async_copy(rrows_hbm, rrows, l_sem.at[0]),
        pltpu.make_async_copy(mrows_hbm, mrows, l_sem.at[1]),
        pltpu.make_async_copy(win_hbm, win, l_sem.at[2]),
        pltpu.make_async_copy(wgi_hbm, wgi, l_sem.at[3]),
        pltpu.make_async_copy(wgo_hbm, wgo, l_sem.at[4]),
        pltpu.make_async_copy(eg_hbm.at[0], wgu.at[:, pl.ds(0, FW)], l_sem.at[5]),
        pltpu.make_async_copy(eu_hbm.at[0], wgu.at[:, pl.ds(2 * FW, FW)], l_sem.at[6]),
        pltpu.make_async_copy(ed_hbm.at[0], wd.at[pl.ds(0, FW), :], l_sem.at[7]),
        pltpu.make_async_copy(wmo_hbm, wmo.at[pl.ds(0, HC), :], l_sem.at[8]),
        pltpu.make_async_copy(ids_hbm, ids_ref, l_sem.at[9]),
        pltpu.make_async_copy(rw_hbm, rw_ref, l_sem.at[10]),
        pltpu.make_async_copy(rgain_hbm, rgain, l_sem.at[11]),
        pltpu.make_async_copy(mgain_hbm, mgain, l_sem.at[12]),
        pltpu.make_async_copy(taps_hbm, taps, l_sem.at[13]),
    ]
    for i in (9, 0, 11):
        loads[i].start()

    barrier = pltpu.get_barrier_semaphore()

    def greet(i, carry):
        pl.semaphore_signal(barrier, inc=1, device_id=((c + i) % E, t), device_id_type=MESH)
        return carry

    for dev in (partner, ring[0], ring[1]):
        pl.semaphore_signal(barrier, inc=1, device_id=dev, device_id_type=MESH)
    lax.fori_loop(1, E, greet, 0)

    for i in (1, 12, 2, 3, 4, 10, 13, 5, 6, 7, 8):
        loads[i].start()

    def slot_numbers():
        ids = ids_ref[...]
        expert = lax.broadcasted_iota(jnp.int32, (EP, T), 0)
        hit0 = expert == ids[0:1, :]
        hit1 = expert == ids[1:2, :]
        named = jnp.where(hit0 | hit1, 1.0, 0.0).astype(BF)
        r = lax.broadcasted_iota(jnp.int32, (T, T), 0)
        q = lax.broadcasted_iota(jnp.int32, (T, T), 1)
        upper = jnp.where(r < q, 1.0, 0.0).astype(BF)
        before = dot(named, upper)
        row0 = ids[0:1, :].astype(F32) * CAP + jnp.sum(
            jnp.where(hit0, before, 0.0), axis=0, keepdims=True
        )
        row1 = ids[1:2, :].astype(F32) * CAP + jnp.sum(
            jnp.where(hit1, before, 0.0), axis=0, keepdims=True
        )
        return row0, row1

    def slot_columns():
        r = lax.broadcasted_iota(jnp.int32, (T, T), 0)
        q = lax.broadcasted_iota(jnp.int32, (T, T), 1)
        diag = r == q
        rows = (slotrow[0:1, :], slotrow[1:2, :], rw_ref[0:1, :], rw_ref[1:2, :])
        return [jnp.sum(jnp.where(diag, row, 0.0), axis=1, keepdims=True) for row in rows]

    cols_y = pl.ds(pl.multiple_of(y * CW, CW), CW)

    def norm_routed():
        step = 32

        def body(i, carry):
            rows = pl.ds(pl.multiple_of(i * step, step), step)
            v = rrows[rows, :].astype(F32)
            scale = lax.rsqrt(jnp.mean(v * v, axis=-1, keepdims=True) + EPS)
            rscale[rows, :] = jnp.broadcast_to(scale, (step, 128))
            part = rrows[rows, cols_y].astype(F32)
            nrm[rows, :] = (part * scale * rgain[:, cols_y]).astype(BF)
            return carry

        lax.fori_loop(0, T // step, body, 0)

    loads[9].wait()

    SC = NS // 4

    def cap_rows(i):
        return pl.ds(pl.multiple_of(i * CAP, CAP), CAP)

    def far(q, i):
        g = far_off[q]
        ze = (z + g) % Z
        xe = (x + i) % X
        row = far_off.index(Z - g) * (X // 2) + x // 2
        return remote(
            xs.at[cap_rows(q * X + xe), :],
            xb.at[y, cap_rows(row), :],
            a2a_s.at[0],
            a2a_r.at[far_off.index(Z - g)],
            (ze * X + xe, t),
        )

    def near(n, i):
        ze = (z + Z + near_off[n]) % Z
        xe = (x + i) % X
        row = (NN - 1 - n) * (X // 2) + x // 2
        return remote(
            xsn.at[cap_rows(n * X + xe), :],
            xn.at[cap_rows(row), :],
            a2a_s.at[1],
            a2a_r.at[NF],
            (ze * X + xe, t),
        )

    own_row = NW * (X // 2) + x // 2
    near_order = [n for n in range(NN) if n != NW] + [NW]

    def pick_plane(zp):
        number = lax.broadcasted_iota(jnp.int32, (PS, T), 0) + zp * PS
        row0 = slotrow[0:1, :].astype(jnp.int32)
        row1 = slotrow[1:2, :].astype(jnp.int32)
        return jnp.where((number == row0) | (number == row1), 1.0, 0.0).astype(BF)

    @pl.when(active)
    def _():
        row0, row1 = slot_numbers()
        loads[0].wait()
        loads[11].wait()
        norm_routed()
        slotrow[0:1, :] = row0
        slotrow[1:2, :] = row1

        def select(q):
            pick = pick_plane((z + far_off[q]) % Z)
            xs[q * PS : (q + 1) * PS, :] = dot(pick, nrm[...]).astype(BF)

        for q in range(NF):
            select(q)

    @pl.when(jnp.logical_not(active))
    def _():
        for i in (0, 10, 11):
            loads[i].wait()

    pl.semaphore_wait(barrier, E + 2)

    @pl.when(active)
    def _():
        for q in range(NF):

            def send_far(i, carry):
                far(q, i).start()
                return carry

            lax.fori_loop(0, X, send_far, 0)

    weights = [
        remote(eg_hbm.at[0], wgu.at[:, pl.ds(FW, FW)], wt_s.at[0], wt_r.at[0], partner),
        remote(eu_hbm.at[0], wgu.at[:, pl.ds(3 * FW, FW)], wt_s.at[1], wt_r.at[1], partner),
        remote(ed_hbm.at[0], wd.at[pl.ds(FW, FW), :], wt_s.at[2], wt_r.at[2], partner),
        remote(wmo_hbm, wmo.at[pl.ds(HC, HC), :], wt_s.at[3], wt_r.at[3], partner),
    ]
    for one in weights:
        one.start()

    for i in (1, 2, 3, 4, 12, 13):
        loads[i].wait()

    def norm_mixer(i, carry):
        rows = pl.ds(pl.multiple_of(i * 16, 16), 16)
        v = mrows[rows, :].astype(F32)
        scale = lax.rsqrt(jnp.mean(v * v, axis=-1, keepdims=True) + EPS)
        mn[rows, :] = (v * scale * mgain[...]).astype(BF)
        return carry

    lax.fori_loop(0, M // 16, norm_mixer, 0)
    normed = mn[...]
    inner = dot_t(normed, win[...])
    gate_in = dot_t(normed, wgi[...])
    go[:, 0:HC] = dot_t(normed, wgo[...])
    ci[...] = jnp.zeros(ci.shape, BF)
    ci[:, 0:HC] = (gate_in * inner).astype(BF)
    send_halo = remote(ci.at[pl.ds(M - 16, 16), :], halo, halo_s, halo_r, ((c + 1) % E, t))
    send_halo.start()

    @pl.when(active)
    def _():
        def norm_full(i, carry):
            rows = pl.ds(pl.multiple_of(i * 16, 16), 16)
            v = rrows[rows, :].astype(F32)
            nfull[rows, :] = (v * rscale[rows, 0:1] * rgain[...]).astype(BF)
            return carry

        lax.fori_loop(0, T // 16, norm_full, 0)

        for n in near_order:
            pick = pick_plane((z + Z + near_off[n]) % Z)
            xsn[n * PS : (n + 1) * PS, :] = dot(pick, nfull[...]).astype(BF)

            def send_near(i, carry):
                near(n, i).start()
                return carry

            lax.fori_loop(1 if n == NW else 0, X, send_near, 0)
        xn[cap_rows(own_row), :] = xsn[cap_rows(NW * X + x), :]

        loads[10].wait()
        s0, s1, w0, w1 = slot_columns()
        s0 = s0.astype(jnp.int32)
        s1 = s1.astype(jnp.int32)
        for i in range(4):
            number = lax.broadcasted_iota(jnp.int32, (T, SC), 1) + i * SC
            w = jnp.where(number == s0, w0, 0.0) + jnp.where(number == s1, w1, 0.0)
            top = w.astype(BF)
            whi[:, i * SC : (i + 1) * SC] = top
            wlo[:, i * SC : (i + 1) * SC] = (w - top.astype(F32)).astype(BF)

    def ag_part(blk, d, s, q):
        if s < S:
            return xb.at[blk, pl.ds(q * QS, QS), :]
        return xb.at[blk, pl.ds(q * QS + d * (QS // 2), QS // 2), :]

    def ag(d, s, q, incoming):
        ref = ag_part((y + Y - sign[d] * (s if incoming else s - 1)) % Y, d, s, q)
        return remote(ref, ref, ag_s, ag_r.at[d, s - 1, q], ring[d])

    def gate_up(blk):
        return dot(xb[blk], wgu[pl.ds(pl.multiple_of(blk * CW, CW), CW), :])

    def near_arrived():
        @pl.when(active)
        def _():
            settle(xn.at[pl.ds(0, RN - CAP), :], a2a_r.at[NF])

        @pl.when(jnp.logical_not(active))
        def _():
            settle(xn, a2a_r.at[NF])

    def finish(both, rows):
        g = both[:, 0 : 2 * FW]
        hid[rows, :] = (g / (1.0 + jnp.exp(-g)) * both[:, 2 * FW :]).astype(BF)

    def columns_of(dest, half):
        return pl.ds(pl.multiple_of(dest * CW + half * CH, CH), CH)

    def mixer_partial(dest):
        cols = pl.ds(pl.multiple_of(dest * CW, CW), CW)
        mine = gsc[pl.ds(pl.multiple_of(k * MH, MH), MH), :]
        return dot(mine[:, 0:HC], wmo[0:HC, cols]) + dot(gpart[:, 0:HC], wmo[HC:, cols])

    def mx(d, s):
        rows = slice(d * MQ, (d + 1) * MQ) if s == 1 else slice(0, MH)
        rows = pl.ds(rows.start, rows.stop - rows.start)
        return remote(
            msbuf.at[d, s - 1, rows, :], mrbuf.at[d, s - 1, rows, :], mx_s, mx_r.at[d, s - 1], ring[d]
        )

    def mx_step(s):
        for d in range(2):
            b = mixer_partial((y + Y + sign[d] * (S + 1 - s)) % Y)
            msbuf[d, s - 1] = b.astype(BF)
            late = slice(d * MQ, (d + 1) * MQ)
            if s > 1:
                mx(d, s - 1).wait_recv()
                rows = late if s == 2 else slice(0, MH)
                msbuf[d, s - 1, rows, :] = (b[rows] + mrbuf[d, s - 2, rows, :].astype(F32)).astype(BF)
            mx(d, s).start()

    def mx_total():
        b = mixer_partial(y)
        for d in range(2):
            mx(d, S).wait_recv()
            b = b + mrbuf[d, S - 1].astype(F32)
        mout[pl.ds(pl.multiple_of(k * MH, MH), MH), cols_y] = b.astype(BF)

    mixer_steps = [functools.partial(mx_step, s) for s in range(1, S + 1)] + [mx_total]

    def mixer_on():
        if mixer_steps:
            mixer_steps.pop(0)()

    def partial(q, dest):
        return dot(hid[q % 2 * RH : (q % 2 + 1) * RH, :], wd[:, columns_of(dest, q // 2)])

    def slot(d, s, q):
        return d * 2 + q // 2 if s == 1 else 4 + ((s - 2) * 2 + d) * 4 + q

    def rs(d, s, q):
        i = slot(d, s, q)
        return remote(sbuf.at[i], rbuf.at[i], rs_s, rs_r.at[i], ring[d])

    def rs_step(d, s, q):
        a = partial(q, (y + Y + sign[d] * (S + 1 - s)) % Y)
        if s > 2 or (s == 2 and q % 2 == d):
            rs(d, s - 1, q).wait_recv()
            a = a + rbuf[slot(d, s - 1, q)].astype(F32)
        sbuf[slot(d, s, q)] = a.astype(BF)
        rs(d, s, q).start()

    for s in range(1, S + 2):
        for q in range(NF):
            if s == 1:
                settle(xb.at[y, pl.ds(q * QS, QS), :], a2a_r.at[q])
            for d in range(2):
                if s > 1:
                    ag(d, s - 1, q, True).wait_recv()
                if s <= S:
                    ag(d, s, q, False).start()
            if s == 2 and q == 0:
                for i in (5, 6):
                    loads[i].wait()
                weights[0].wait_recv()
                weights[1].wait_recv()
                acc[...] = gate_up(y)
            if s > 2 and q == 0:
                acc[...] += gate_up((y + Y - s + 2) % Y)
            if s > 2 and q == NF // 2:
                acc[...] += gate_up((y + s - 2) % Y)
        if s == S + 1:
            finish(acc[...] + gate_up((y + S) % Y), slice(0, RF))
        if s == S:
            loads[8].wait()
            weights[3].wait_recv()
            send_g.wait_recv()
            near_arrived()
            finish(dot(xn[...], wgu[...]), slice(RF, R))
            mixer_on()
            loads[7].wait()
            weights[2].wait_recv()
        if s == S - 1:
            send_halo.wait_recv()
            ext[0:16, :] = jnp.where(c > 0, halo[...].astype(F32), 0.0)
            ext[16:, :] = ci[...].astype(F32)
            conv = taps[0:1, :] * ext[14 : 14 + M, 0:HC]
            conv = conv + taps[1:2, :] * ext[15 : 15 + M, 0:HC]
            conv = conv + taps[2:3, :] * ext[16 : 16 + M, 0:HC]
            gsc[...] = jnp.zeros(gsc.shape, BF)
            gsc[:, 0:HC] = (go[:, 0:HC] * conv).astype(BF)
            send_g = remote(
                gsc.at[pl.ds(pl.multiple_of((1 - k) * MH, MH), MH), :], gpart, g_s, g_r, partner
            )
            send_g.start()

    turns = [(0, 1), (1, 2), (2, 1), (3, 2)]
    for s in range(2, S):
        turns += [(0, s), (1, s + 1), (2, s), (3, s + 1)]
    turns += [(0, S), (2, S)]
    for n, (q, s) in enumerate(turns):
        for d in range(2):
            rs_step(d, s, q ^ d)
        if n % 4 == 1:
            mixer_on()
    while mixer_steps:
        mixer_on()

    def mixer_piece(core, rel, h):
        cols = pl.ds(pl.multiple_of(((y + Y + rel) % Y) * CW, CW), CW)
        if h is None:
            return mout.at[pl.ds(pl.multiple_of(core * MH, MH), MH), cols]
        return mout.at[pl.ds(pl.multiple_of(core * MH + h * MQ, MQ), MQ), cols]

    def mg(d, s, incoming):
        ref = mixer_piece(k, -sign[d] * (s if incoming else s - 1), None if s < S else d)
        return remote(ref, ref, mg_s, mg_r.at[d, s - 1], ring[d])

    mixer_pieces = [(0, None)]
    for s in range(1, S):
        mixer_pieces += [(-s, None), (s, None)]
    mixer_pieces += [(S, 0), (S, 1)]

    def md(i, core):
        ref = mixer_piece(core, *mixer_pieces[i])
        return remote(ref, ref, md_s, md_r, partner)

    def mg_on(s):
        for d in range(2):
            if s > 1:
                mg(d, s - 1, True).wait_recv()
            if s <= S:
                mg(d, s, False).start()
            if s > 1:
                md(1 + (s - 2) * 2 + d, k).start()

    mg_on(1)
    md(0, k).start()

    def target(i):
        zc = (z + Z + order_off[i // (X // 2)]) % Z
        return zc * X + i % (X // 2) * 2 + k

    def giving(i, half):
        return remote(
            fin.at[half, pl.ds(i * CAP, CAP), :],
            ret.at[half, cap_rows(c), :],
            ret_s,
            ret_r.at[half],
            (target(i), t),
        )

    def distance(i):
        g = order_off[i // (X // 2)] % Z
        return min(g, Z - g)

    own = [i for i in range(E // 2) if order_off[i // (X // 2)] == 0]

    def unless_own(i, act):
        if i in own:
            pl.when(target(i) != c)(act)
        else:
            act()

    def total(q):
        a = partial(q, y)
        for d in range(2):
            rs(d, S, q).wait_recv()
            a = a + rbuf[slot(d, S, q)].astype(F32)
        half, rows = q // 2, q % 2
        fin[half, rows * RH : (rows + 1) * RH, :] = a.astype(BF)
        for i in sorted(range(rows * E // 4, (rows + 1) * E // 4), key=distance, reverse=True):
            unless_own(i, lambda: giving(i, half).start())

    total(0)
    total(1)

    total(2)
    total(3)
    mg_on(2)

    @pl.when(active)
    def _():
        for half in range(2):
            ret[half, cap_rows(c), :] = fin[half, cap_rows(own[0] + x // 2), :]

    def routed_piece(rel, h):
        return rout.at[pl.ds(h % 2 * (T // 2), T // 2), columns_of((y + Y + rel) % Y, h // 2)]

    def pieces(j):
        return [(d, h) for h in range(4) for d in range(2) if j < S or h % 2 == d]

    def rg(d, j, h, incoming):
        if incoming:
            ref = routed_piece(-sign[d] * j, h)
        else:
            ref = routed_piece(0 if j <= 2 else -sign[d] * 2, h)
        dev = (c, ((y + Y + sign[d] * (j if j <= 2 else j - 2)) % Y) * 2 + k)
        return remote(ref, ref, rg_s, ag_r.at[d, j - 1, h], dev)

    def rd(d, j, h):
        ref = routed_piece(-sign[d] * j, h)
        return remote(ref, ref, rd_s, rd_r, partner)

    @pl.when(active)
    def _():
        for half in range(2):

            settle(ret.at[half, pl.ds(0, NS - CAP), :], ret_r.at[half])
            for h in range(2):
                rows = slice(h * (T // 2), (h + 1) * (T // 2))
                weighted = dot(whi[rows, :], ret[half]) + dot(wlo[rows, :], ret[half])
                rout[rows, columns_of(y, half)] = weighted.astype(BF)
                for d, i in pieces(2):
                    if i == 2 * half + h:
                        rg(d, 2, i, False).start()
                rd(0, 0, 2 * half + h).start()
            for d, i in pieces(1):
                if i // 2 == half:
                    rg(d, 1, i, False).start()
        for half in range(2):
            mg_on(3 + half)
            for d, h in pieces(2):
                if h // 2 == half:
                    rg(d, 2, h, True).wait_recv()
                    for j in range(S, 2, -1):
                        if (d, h) in pieces(j):
                            rg(d, j, h, False).start()
                    rd(d, 2, h).start()
        for half in range(2):
            for j in [1] + list(range(3, S + 1)):
                for d, h in pieces(j):
                    if h // 2 == half:
                        rg(d, j, h, True).wait_recv()
                        rd(d, j, h).start()
        for s in range(5, S + 2):
            mg_on(s)

    @pl.when(jnp.logical_not(active))
    def _():
        for s in range(3, S + 2):
            mg_on(s)

    settle(mout.at[pl.ds(0, MH), :], md_s)
    settle(mout.at[pl.ds(0, MH), :], md_r)
    settle(mout.at[pl.ds(0, MH), pl.ds(0, D - CW)], mg_s)
    settle(mout.at[pl.ds(0, MH), pl.ds(0, D - CW)], mx_s)
    settle(xb.at[pl.ds(0, Y - 1)], ag_s)
    settle(sbuf, rs_s)
    for one in weights:
        one.wait_send()
    send_halo.wait_send()
    send_g.wait_send()
    @pl.when(active)
    def _():
        settle(fin.at[:, pl.ds(0, R - CAP), :], ret_s)
        settle(xs, a2a_s.at[0])
        settle(xsn.at[pl.ds(0, NN * PS - CAP), :], a2a_s.at[1])
        settle(rout.at[:, pl.ds(0, D - CW)], rg_s)
        settle(rout, rd_s)

    @pl.when(jnp.logical_not(active))
    def _():
        settle(fin, ret_s)
        settle(rout, rd_r)


def on_device(E, Y, mrows, mgain, win, wgi, wgo, taps, wmo, rrows, rgain, ids, rw, eg, eu, ed):
    M, D = mrows.shape
    T = rrows.shape[0]
    HC = win.shape[1]
    FW = eg.shape[2]
    CW = D // Y
    S = Y // 2
    CAP = 2 * T * ids.shape[1] // E
    X = 4
    NW = 1 if E // X > 3 else 0
    NF = E // X - 2 * NW - 1
    R = E * CAP // 2
    RN = (2 * NW + 1) * (X // 2) * CAP
    VM = pl.BlockSpec(memory_space=pltpu.VMEM)
    HB = pl.BlockSpec(memory_space=pl.ANY)
    DS = pltpu.SemaphoreType.DMA
    return pl.pallas_call(
        functools.partial(kernel, E, Y, X, NW, CAP),
        out_shape=(pltpu.VMEM((M, D), BF), pltpu.VMEM((T, D), BF)),
        in_specs=[HB] * 14,
        out_specs=(VM, VM),
        scratch_shapes=[
            pltpu.VMEM((1, D), F32),
            pltpu.VMEM(taps.shape, F32),
            pltpu.VMEM((1, D), F32),
            pltpu.VMEM((2, T), jnp.int32),
            pltpu.VMEM((2, T), F32),
            pltpu.VMEM((M, D), BF),
            pltpu.VMEM((M, D), BF),
            pltpu.VMEM((HC, D), BF),
            pltpu.VMEM((HC, D), BF),
            pltpu.VMEM((HC, D), BF),
            pltpu.VMEM((2 * HC, D), BF),
            pltpu.VMEM((T, D), BF),
            pltpu.VMEM((T, CW), BF),
            pltpu.VMEM((T, D), BF),
            pltpu.VMEM((T, 128), F32),
            pltpu.VMEM((D, 4 * FW), BF),
            pltpu.VMEM((2 * FW, D), BF),
            pltpu.VMEM((8, T), F32),
            pltpu.VMEM(((R - RN) * 2, CW), BF),
            pltpu.VMEM((2 * RN, D), BF),
            pltpu.VMEM((Y, R - RN, CW), BF),
            pltpu.VMEM((RN, D), BF),
            pltpu.VMEM((R - RN, 4 * FW), F32),
            pltpu.VMEM((R, 2 * FW), BF),
            pltpu.VMEM((8 * S - 4, R // 2, CW // 2), BF),
            pltpu.VMEM((8 * S - 4, R // 2, CW // 2), BF),
            pltpu.VMEM((2, S, M // 2, CW), BF),
            pltpu.VMEM((2, S, M // 2, CW), BF),
            pltpu.VMEM((2, R, CW // 2), BF),
            pltpu.VMEM((2, E * CAP, CW // 2), BF),
            pltpu.VMEM((T, E * CAP), BF),
            pltpu.VMEM((T, E * CAP), BF),
            pltpu.VMEM((M, 128), BF),
            pltpu.VMEM((16, 128), BF),
            pltpu.VMEM((M + 16, 128), F32),
            pltpu.VMEM((M, 128), F32),
            pltpu.VMEM((M, 128), BF),
            pltpu.VMEM((M // 2, 128), BF),
            DS((14,)),
            DS((4,)),
            DS((4,)),
            DS((2,)),
            DS((NF + 1,)),
            DS,
            DS,
            DS,
            DS,
            DS,
            DS((2, S, max(NF, 4))),
            DS,
            DS((8 * S - 4,)),
            DS,
            DS((2, S)),
            DS,
            DS((2,)),
            DS,
            DS((2, S)),
            DS,
            DS,
            DS,
            DS,
            DS,
        ],
        compiler_params=pltpu.CompilerParams(collective_id=0, has_side_effects=True),
    )(
        mrows,
        mgain.reshape(1, D),
        win.T,
        wgi.T,
        wgo.T,
        taps,
        wmo,
        rrows,
        rgain.reshape(1, D),
        ids.T,
        rw.T,
        eg,
        eu,
        ed,
    )


def solution(mesh):
    E = mesh.shape["ep"]
    Y = mesh.shape["tp"] // 2
    return jax.shard_map(
        functools.partial(on_device, E, Y),
        mesh=mesh,
        in_specs=(
            P("ep", None),
            P(),
            P(None, "tp"),
            P(None, "tp"),
            P(None, "tp"),
            P(None, "tp"),
            P("tp", None),
            P("ep", None),
            P(),
            P("ep", None),
            P("ep", None),
            P("ep", None, "tp"),
            P("ep", None, "tp"),
            P("ep", "tp", None),
        ),
        out_specs=(P("ep", None), P("ep", None)),
        check_vma=False,
    )
```

time: 95.8 us -> 86.4 us (0.902)
  Pallas kernels: 93.2 us -> 83.8 us
    pallas_call x1, Pallas kernels: 93.2 us -> 83.8 us  [on_device(): pl.pallas_call(functools.partial(kernel, E, Y, X, NW, CAP), out_shape=(pl...]
where the time goes in v3:
time: 86.4 us; the launch traced here: 86.2 us
  Pallas kernels  83.8 us (97%)
  local copies, waits for them, and re-layouts  1.77 us (2%)
    pallas_call x1, Pallas kernels, on_device(): pl.pallas_call(functools.partial(kernel, E, Y, X, NW, CAP), out_shape=(pl...  83.8 us
    unnamed x2, local copies, waits for them, and re-layouts  1.77 us

profile of v3, /device:TPU:1, one launch (start us, length us, event | category | flops | bytes accessed | tf_op | source)
XLA Modules:
  0.0 86.2 jit_solution(964975767297372351)
XLA Ops:
  0.6 83.8 %shard_map.149 = (bf16[128,2048]{1,0:T(8,128)(2,1)S(1)}, bf16[256,2048]{1,0:T(8,128)(2,1)S(1)}) custom-call(bf16[128,2048]{1,0:T(8,128)(2,1)} %mrows_hbm.1, f32[1,2048]{1,0:T(1,128)} %bitcast.10, bf16[64,2048]{1,0:T(8,128)(2,1)} %bitcast.7, bf16[64,2048]{1,0:T(8,128)(2,1)} %bitcast.8, bf16[64,2048]{1,0:T(8,128)(2,1)} %bitcast.9, f32[3,64]{1,0:T(4,128)} %taps_hbm.1, ...), custom_call_target="tpu_custom_call" | custom-call | tf_op jit(solution)/shard_map/pallas_call | solution.py:674
  84.5 0.8 copy.18
  85.3 1.0 %copy.19 = bf16[256,2048]{1,0:T(8,128)(2,1)} copy(bf16[256,2048]{1,0:T(8,128)(2,1)S(1)} %get-tuple-element.3) | data formatting | bytes 2097152

commit v4 on v3

--- a/solution.py
+++ b/solution.py
@@ -17,6 +17,15 @@
     return jnp.dot(a, b, preferred_element_type=F32)
 
 
+def plan(Z):
+    every = [(g, u) for g in sorted(range(Z), key=lambda g: min(g, Z - g)) for u in range(2)]
+    reach = 1 if Z > 4 else 0
+    near = [b for b in every if min(b[0], Z - b[0]) <= reach]
+    if reach:
+        near += [(2, 0), (Z - 2, 0)]
+    return near, sorted([b for b in every if b not in near], key=lambda b: min(b[0], Z - b[0]))
+
+
 def dot_t(a, b):
     return lax.dot_general(a, b, (((1,), (1,)), ((), ())), preferred_element_type=F32)
 
@@ -25,7 +34,6 @@
     E,
     Y,
     X,
-    NW,
     CAP,
     mrows_hbm,
     mgain_hbm,
@@ -120,17 +128,12 @@
     NS = E * CAP
     R = NS // 2
     Z = E // X
-    NN = 2 * NW + 1
-    NF = Z - NN
-    PS = X * CAP
-    NP = NN * X // 2
-    FP = NF * X // 2
-    RN = NP * CAP
-    RF = FP * CAP
-    QS = PS // 2
-    near_off = list(range(-NW, NW + 1))
-    far_off = sorted(range(NW + 1, Z - NW), key=lambda g: min(g, Z - g))
-    order_off = far_off + near_off
+    near_blocks, far_blocks = plan(Z)
+    blocks = near_blocks + far_blocks
+    NF = len(far_blocks) // 2
+    RN = len(near_blocks) * CAP
+    RF = len(far_blocks) * CAP
+    QS = 2 * CAP
     RH = R // 2
     CH = CW // 2
     MH = M // 2
@@ -171,13 +174,16 @@
 
     barrier = pltpu.get_barrier_semaphore()
 
-    def greet(i, carry):
-        pl.semaphore_signal(barrier, inc=1, device_id=((c + i) % E, t), device_id_type=MESH)
-        return carry
-
+    for g in sorted(range(Z), key=lambda g: -min(g, Z - g)):
+
+        def greet(i, carry):
+            there = (z + g) % Z * X + (x + i) % X
+            pl.semaphore_signal(barrier, inc=1, device_id=(there, t), device_id_type=MESH)
+            return carry
+
+        lax.fori_loop(0 if g else 1, X, greet, 0)
     for dev in (partner, ring[0], ring[1]):
         pl.semaphore_signal(barrier, inc=1, device_id=dev, device_id_type=MESH)
-    lax.fori_loop(1, E, greet, 0)
 
     for i in (1, 12, 2, 3, 4, 10, 13, 5, 6, 7, 8):
         loads[i].start()
@@ -230,39 +236,37 @@
     def cap_rows(i):
         return pl.ds(pl.multiple_of(i * CAP, CAP), CAP)
 
-    def far(q, i):
-        g = far_off[q]
-        ze = (z + g) % Z
-        xe = (x + i) % X
-        row = far_off.index(Z - g) * (X // 2) + x // 2
+    def there(g, u, i):
+        return (z + Z - g) % Z * X + (x // 2 ^ u) * 2 + i
+
+    def far(b, i):
         return remote(
-            xs.at[cap_rows(q * X + xe), :],
-            xb.at[y, cap_rows(row), :],
+            xs.at[cap_rows(2 * b + i), :],
+            xb.at[y, pl.ds(b * CAP, CAP), :],
             a2a_s.at[0],
-            a2a_r.at[far_off.index(Z - g)],
-            (ze * X + xe, t),
+            a2a_r.at[b // 2],
+            (there(*far_blocks[b], i), t),
         )
 
-    def near(n, i):
-        ze = (z + Z + near_off[n]) % Z
-        xe = (x + i) % X
-        row = (NN - 1 - n) * (X // 2) + x // 2
+    def near(b, i):
         return remote(
-            xsn.at[cap_rows(n * X + xe), :],
-            xn.at[cap_rows(row), :],
+            xsn.at[cap_rows(2 * b + i), :],
+            xn.at[pl.ds(b * CAP, CAP), :],
             a2a_s.at[1],
             a2a_r.at[NF],
-            (ze * X + xe, t),
+            (there(*near_blocks[b], i), t),
         )
 
-    own_row = NW * (X // 2) + x // 2
-    near_order = [n for n in range(NN) if n != NW] + [NW]
-
-    def pick_plane(zp):
-        number = lax.broadcasted_iota(jnp.int32, (PS, T), 0) + zp * PS
+    OWN = near_blocks.index((0, 0))
+
+    def pick(group):
         row0 = slotrow[0:1, :].astype(jnp.int32)
         row1 = slotrow[1:2, :].astype(jnp.int32)
-        return jnp.where((number == row0) | (number == row1), 1.0, 0.0).astype(BF)
+        parts = []
+        for g, u in group:
+            number = lax.broadcasted_iota(jnp.int32, (2 * CAP, T), 0) + there(g, u, 0) * CAP
+            parts.append(jnp.where((number == row0) | (number == row1), 1.0, 0.0).astype(BF))
+        return jnp.concatenate(parts, axis=0)
 
     @pl.when(active)
     def _():
@@ -273,12 +277,7 @@
         slotrow[0:1, :] = row0
         slotrow[1:2, :] = row1
 
-        def select(q):
-            pick = pick_plane((z + far_off[q]) % Z)
-            xs[q * PS : (q + 1) * PS, :] = dot(pick, nrm[...]).astype(BF)
-
-        for q in range(NF):
-            select(q)
+        xs[...] = dot(pick(far_blocks), nrm[...]).astype(BF)
 
     @pl.when(jnp.logical_not(active))
     def _():
@@ -289,13 +288,9 @@
 
     @pl.when(active)
     def _():
-        for q in range(NF):
-
-            def send_far(i, carry):
-                far(q, i).start()
-                return carry
-
-            lax.fori_loop(0, X, send_far, 0)
+        for b in range(len(far_blocks)):
+            for i in range(2):
+                far(b, i).start()
 
     weights = [
         remote(eg_hbm.at[0], wgu.at[:, pl.ds(FW, FW)], wt_s.at[0], wt_r.at[0], partner),
@@ -336,16 +331,17 @@
 
         lax.fori_loop(0, T // 16, norm_full, 0)
 
-        for n in near_order:
-            pick = pick_plane((z + Z + near_off[n]) % Z)
-            xsn[n * PS : (n + 1) * PS, :] = dot(pick, nfull[...]).astype(BF)
-
-            def send_near(i, carry):
-                near(n, i).start()
-                return carry
-
-            lax.fori_loop(1 if n == NW else 0, X, send_near, 0)
-        xn[cap_rows(own_row), :] = xsn[cap_rows(NW * X + x), :]
+        for first in range(0, len(near_blocks), 4):
+            group = near_blocks[first : first + 4]
+            rows = slice(2 * first * CAP, 2 * (first + len(group)) * CAP)
+            xsn[rows, :] = dot(pick(group), nfull[...]).astype(BF)
+        for b in range(len(near_blocks) - 1, -1, -1):
+            for i in range(2):
+                if b == OWN:
+                    pl.when(x % 2 != i)(lambda: near(b, i).start())
+                else:
+                    near(b, i).start()
+        xn[OWN * CAP : (OWN + 1) * CAP, :] = xsn[cap_rows(2 * OWN + x % 2), :]
 
         loads[10].wait()
         s0, s1, w0, w1 = slot_columns()
@@ -367,8 +363,8 @@
         ref = ag_part((y + Y - sign[d] * (s if incoming else s - 1)) % Y, d, s, q)
         return remote(ref, ref, ag_s, ag_r.at[d, s - 1, q], ring[d])
 
-    def gate_up(blk):
-        return dot(xb[blk], wgu[pl.ds(pl.multiple_of(blk * CW, CW), CW), :])
+    def gate_up(blk, rows=slice(None)):
+        return dot(xb[blk, rows, :], wgu[pl.ds(pl.multiple_of(blk * CW, CW), CW), :])
 
     def near_arrived():
         @pl.when(active)
@@ -440,49 +436,72 @@
         sbuf[slot(d, s, q)] = a.astype(BF)
         rs(d, s, q).start()
 
-    for s in range(1, S + 2):
-        for q in range(NF):
-            if s == 1:
-                settle(xb.at[y, pl.ds(q * QS, QS), :], a2a_r.at[q])
-            for d in range(2):
-                if s > 1:
-                    ag(d, s - 1, q, True).wait_recv()
-                if s <= S:
-                    ag(d, s, q, False).start()
-            if s == 2 and q == 0:
-                for i in (5, 6):
-                    loads[i].wait()
-                weights[0].wait_recv()
-                weights[1].wait_recv()
-                acc[...] = gate_up(y)
-            if s > 2 and q == 0:
-                acc[...] += gate_up((y + Y - s + 2) % Y)
-            if s > 2 and q == NF // 2:
-                acc[...] += gate_up((y + s - 2) % Y)
-        if s == S + 1:
-            finish(acc[...] + gate_up((y + S) % Y), slice(0, RF))
-        if s == S:
+    def mixer_rest():
+        send_halo.wait_recv()
+        ext[0:16, :] = jnp.where(c > 0, halo[...].astype(F32), 0.0)
+        ext[16:, :] = ci[...].astype(F32)
+        conv = taps[0:1, :] * ext[14 : 14 + M, 0:HC]
+        conv = conv + taps[1:2, :] * ext[15 : 15 + M, 0:HC]
+        conv = conv + taps[2:3, :] * ext[16 : 16 + M, 0:HC]
+        gsc[...] = jnp.zeros(gsc.shape, BF)
+        gsc[:, 0:HC] = (go[:, 0:HC] * conv).astype(BF)
+        send_g = remote(
+            gsc.at[pl.ds(pl.multiple_of((1 - k) * MH, MH), MH), :], gpart, g_s, g_r, partner
+        )
+        send_g.start()
+        return send_g
+
+    def own_products():
+        for i in (5, 6):
+            loads[i].wait()
+        weights[0].wait_recv()
+        weights[1].wait_recv()
+        acc[...] = gate_up(y)
+
+    def products(rel):
+        acc[...] += gate_up((y + Y + rel) % Y)
+
+    hop = 2.75
+    steps = [(s, q) for s in range(1, S + 1) for q in range(NF)]
+    steps.sort(key=lambda one: (one[1] + hop * (one[0] - 1), -one[0]))
+    waiting = []
+    for s, q in steps:
+        if s == 1:
+            settle(xb.at[y, pl.ds(q * QS, QS), :], a2a_r.at[q])
+        else:
+            pass
+        for d in range(2):
+            if s > 1:
+                ag(d, s - 1, q, True).wait_recv()
+            ag(d, s, q, False).start()
+        if q == NF - 1:
+            waiting += [own_products] if s == 1 else [
+                functools.partial(products, s - 1),
+                functools.partial(products, 1 - s),
+            ]
+        if waiting:
+            waiting.pop(0)()
+        if (s, q) == (2, 0):
+            send_g = mixer_rest()
             loads[8].wait()
+        if (s, q) == (2, min(1, NF - 1)):
             weights[3].wait_recv()
             send_g.wait_recv()
-            near_arrived()
-            finish(dot(xn[...], wgu[...]), slice(RF, R))
+        if (s, q) in ((2, min(1, NF - 1)), (3, 2), (4, 3)):
             mixer_on()
-            loads[7].wait()
-            weights[2].wait_recv()
-        if s == S - 1:
-            send_halo.wait_recv()
-            ext[0:16, :] = jnp.where(c > 0, halo[...].astype(F32), 0.0)
-            ext[16:, :] = ci[...].astype(F32)
-            conv = taps[0:1, :] * ext[14 : 14 + M, 0:HC]
-            conv = conv + taps[1:2, :] * ext[15 : 15 + M, 0:HC]
-            conv = conv + taps[2:3, :] * ext[16 : 16 + M, 0:HC]
-            gsc[...] = jnp.zeros(gsc.shape, BF)
-            gsc[:, 0:HC] = (go[:, 0:HC] * conv).astype(BF)
-            send_g = remote(
-                gsc.at[pl.ds(pl.multiple_of((1 - k) * MH, MH), MH), :], gpart, g_s, g_r, partner
-            )
-            send_g.start()
+    for one in waiting:
+        one()
+    near_arrived()
+    finish(dot(xn[...], wgu[...]), slice(0, RN))
+    early = [(0, 1, 0), (1, 2, 0), (0, 1, 2), (1, 2, 2)]
+    loads[7].wait()
+    weights[2].wait_recv()
+    for one in early:
+        rs_step(*one)
+    for q in range(NF):
+        for d in range(2):
+            ag(d, S, q, True).wait_recv()
+    finish(acc[...] + gate_up((y + S) % Y), slice(RN, R))
 
     turns = [(0, 1), (1, 2), (2, 1), (3, 2)]
     for s in range(2, S):
@@ -490,8 +509,9 @@
     turns += [(0, S), (2, S)]
     for n, (q, s) in enumerate(turns):
         for d in range(2):
-            rs_step(d, s, q ^ d)
-        if n % 4 == 1:
+            if (d, s, q ^ d) not in early:
+                rs_step(d, s, q ^ d)
+        if n in (1, 6):
             mixer_on()
     while mixer_steps:
         mixer_on()
@@ -502,34 +522,30 @@
             return mout.at[pl.ds(pl.multiple_of(core * MH, MH), MH), cols]
         return mout.at[pl.ds(pl.multiple_of(core * MH + h * MQ, MQ), MQ), cols]
 
-    def mg(d, s, incoming):
-        ref = mixer_piece(k, -sign[d] * (s if incoming else s - 1), None if s < S else d)
-        return remote(ref, ref, mg_s, mg_r.at[d, s - 1], ring[d])
-
-    mixer_pieces = [(0, None)]
-    for s in range(1, S):
-        mixer_pieces += [(-s, None), (s, None)]
-    mixer_pieces += [(S, 0), (S, 1)]
-
-    def md(i, core):
-        ref = mixer_piece(core, *mixer_pieces[i])
+    def mg(d, j, incoming):
+        h = None if j < S else d
+        if incoming:
+            ref = mixer_piece(k, -sign[d] * j, h)
+        else:
+            ref = mixer_piece(k, 0 if j <= 2 else -sign[d] * 2, h)
+        dev = (c, ((y + Y + sign[d] * (j if j <= 2 else j - 2)) % Y) * 2 + k)
+        return remote(ref, ref, mg_s, mg_r.at[d, j - 1], dev)
+
+    def md(d, j):
+        ref = mixer_piece(k, -sign[d] * j, None if j < S else d)
         return remote(ref, ref, md_s, md_r, partner)
 
-    def mg_on(s):
+    def mixer_arrived(j):
         for d in range(2):
-            if s > 1:
-                mg(d, s - 1, True).wait_recv()
-            if s <= S:
-                mg(d, s, False).start()
-            if s > 1:
-                md(1 + (s - 2) * 2 + d, k).start()
-
-    mg_on(1)
-    md(0, k).start()
+            mg(d, j, True).wait_recv()
+            if j == 2:
+                for far_j in range(S, 2, -1):
+                    mg(d, far_j, False).start()
+            md(d, j).start()
 
     def target(i):
-        zc = (z + Z + order_off[i // (X // 2)]) % Z
-        return zc * X + i % (X // 2) * 2 + k
+        g, u = blocks[i]
+        return (z + g) % Z * X + (x // 2 ^ u) * 2 + k
 
     def giving(i, half):
         return remote(
@@ -541,13 +557,10 @@
         )
 
     def distance(i):
-        g = order_off[i // (X // 2)] % Z
-        return min(g, Z - g)
-
-    own = [i for i in range(E // 2) if order_off[i // (X // 2)] == 0]
+        return min(blocks[i][0], Z - blocks[i][0])
 
     def unless_own(i, act):
-        if i in own:
+        if i == OWN:
             pl.when(target(i) != c)(act)
         else:
             act()
@@ -567,12 +580,16 @@
 
     total(2)
     total(3)
-    mg_on(2)
+    for j in (2, 1):
+        for d in range(2):
+            mg(d, j, False).start()
+    remote(mixer_piece(k, 0, None), mixer_piece(k, 0, None), md_s, md_r, partner).start()
+    mixer_arrived(2)
 
     @pl.when(active)
     def _():
         for half in range(2):
-            ret[half, cap_rows(c), :] = fin[half, cap_rows(own[0] + x // 2), :]
+            ret[half, cap_rows(c), :] = fin[half, OWN * CAP : (OWN + 1) * CAP, :]
 
     def routed_piece(rel, h):
         return rout.at[pl.ds(h % 2 * (T // 2), T // 2), columns_of((y + Y + rel) % Y, h // 2)]
@@ -609,7 +626,6 @@
                 if i // 2 == half:
                     rg(d, 1, i, False).start()
         for half in range(2):
-            mg_on(3 + half)
             for d, h in pieces(2):
                 if h // 2 == half:
                     rg(d, 2, h, True).wait_recv()
@@ -617,19 +633,19 @@
                         if (d, h) in pieces(j):
                             rg(d, j, h, False).start()
                     rd(d, 2, h).start()
+        for j in [1] + list(range(3, S + 1)):
+            mixer_arrived(j)
         for half in range(2):
             for j in [1] + list(range(3, S + 1)):
                 for d, h in pieces(j):
                     if h // 2 == half:
                         rg(d, j, h, True).wait_recv()
                         rd(d, j, h).start()
-        for s in range(5, S + 2):
-            mg_on(s)
 
     @pl.when(jnp.logical_not(active))
     def _():
-        for s in range(3, S + 2):
-            mg_on(s)
+        for j in [1] + list(range(3, S + 1)):
+            mixer_arrived(j)
 
     settle(mout.at[pl.ds(0, MH), :], md_s)
     settle(mout.at[pl.ds(0, MH), :], md_r)
@@ -645,7 +661,7 @@
     def _():
         settle(fin.at[:, pl.ds(0, R - CAP), :], ret_s)
         settle(xs, a2a_s.at[0])
-        settle(xsn.at[pl.ds(0, NN * PS - CAP), :], a2a_s.at[1])
+        settle(xsn.at[pl.ds(0, 2 * RN - CAP), :], a2a_s.at[1])
         settle(rout.at[:, pl.ds(0, D - CW)], rg_s)
         settle(rout, rd_s)
 
@@ -664,15 +680,15 @@
     S = Y // 2
     CAP = 2 * T * ids.shape[1] // E
     X = 4
-    NW = 1 if E // X > 3 else 0
-    NF = E // X - 2 * NW - 1
+    near_blocks, far_blocks = plan(E // X)
+    NF = len(far_blocks) // 2
     R = E * CAP // 2
-    RN = (2 * NW + 1) * (X // 2) * CAP
+    RN = len(near_blocks) * CAP
     VM = pl.BlockSpec(memory_space=pltpu.VMEM)
     HB = pl.BlockSpec(memory_space=pl.ANY)
     DS = pltpu.SemaphoreType.DMA
     return pl.pallas_call(
-        functools.partial(kernel, E, Y, X, NW, CAP),
+        functools.partial(kernel, E, Y, X, CAP),
         out_shape=(pltpu.VMEM((M, D), BF), pltpu.VMEM((T, D), BF)),
         in_specs=[HB] * 14,
         out_specs=(VM, VM),

time: 86.4 us -> 83.3 us (0.964)
  Pallas kernels: 83.8 us -> 80.8 us
    pallas_call x1, Pallas kernels: 83.8 us -> 80.8 us  [on_device(): pl.pallas_call(functools.partial(kernel, E, Y, X, CAP), out_shape=(pltpu....]
where the time goes in v4:
time: 83.3 us; the launch traced here: 83.2 us
  Pallas kernels  80.8 us (97%)
  local copies, waits for them, and re-layouts  1.77 us (2%)
    pallas_call x1, Pallas kernels, on_device(): pl.pallas_call(functools.partial(kernel, E, Y, X, CAP), out_shape=(pltpu....  80.8 us
    unnamed x2, local copies, waits for them, and re-layouts  1.77 us

profile of v4, /device:TPU:1, one launch (start us, length us, event | category | flops | bytes accessed | tf_op | source)
XLA Modules:
  0.0 83.2 jit_solution(913916628341988806)
XLA Ops:
  0.6 80.8 %shard_map.149 = (bf16[128,2048]{1,0:T(8,128)(2,1)S(1)}, bf16[256,2048]{1,0:T(8,128)(2,1)S(1)}) custom-call(bf16[128,2048]{1,0:T(8,128)(2,1)} %mrows_hbm.1, f32[1,2048]{1,0:T(1,128)} %bitcast.10, bf16[64,2048]{1,0:T(8,128)(2,1)} %bitcast.7, bf16[64,2048]{1,0:T(8,128)(2,1)} %bitcast.8, bf16[64,2048]{1,0:T(8,128)(2,1)} %bitcast.9, f32[3,64]{1,0:T(4,128)} %taps_hbm.1, ...), custom_call_target="tpu_custom_call" | custom-call | tf_op jit(solution)/shard_map/pallas_call | solution.py:690
  81.4 0.8 copy.18
  82.2 1.0 %copy.19 = bf16[256,2048]{1,0:T(8,128)(2,1)} copy(bf16[256,2048]{1,0:T(8,128)(2,1)S(1)} %get-tuple-element.3) | data formatting | bytes 2097152

commit v5 on v4

--- a/solution.py
+++ b/solution.py
@@ -597,12 +597,12 @@
     def pieces(j):
         return [(d, h) for h in range(4) for d in range(2) if j < S or h % 2 == d]
 
+    via = [[0, 0, 0, 2, 2], [0, 0, 0, 2, 0]]
+
     def rg(d, j, h, incoming):
-        if incoming:
-            ref = routed_piece(-sign[d] * j, h)
-        else:
-            ref = routed_piece(0 if j <= 2 else -sign[d] * 2, h)
-        dev = (c, ((y + Y + sign[d] * (j if j <= 2 else j - 2)) % Y) * 2 + k)
+        last = via[h // 2][j]
+        ref = routed_piece(-sign[d] * (j if incoming else last), h)
+        dev = (c, ((y + Y + sign[d] * (j - last)) % Y) * 2 + k)
         return remote(ref, ref, rg_s, ag_r.at[d, j - 1, h], dev)
 
     def rd(d, j, h):
@@ -618,29 +618,23 @@
                 rows = slice(h * (T // 2), (h + 1) * (T // 2))
                 weighted = dot(whi[rows, :], ret[half]) + dot(wlo[rows, :], ret[half])
                 rout[rows, columns_of(y, half)] = weighted.astype(BF)
-                for d, i in pieces(2):
-                    if i == 2 * half + h:
-                        rg(d, 2, i, False).start()
+                for j in (2, 4, 3, 1):
+                    for d, i in pieces(j) if j <= S else []:
+                        if i == 2 * half + h and via[half][j] == 0:
+                            rg(d, j, i, False).start()
                 rd(0, 0, 2 * half + h).start()
-            for d, i in pieces(1):
-                if i // 2 == half:
-                    rg(d, 1, i, False).start()
-        for half in range(2):
-            for d, h in pieces(2):
+        due = [(half, j) for half, j in [(0, 2), (1, 2), (0, 1), (0, 3), (0, 4), (1, 1), (1, 4), (1, 3)] if j <= S]
+        for n, (half, j) in enumerate(due):
+            for d, h in pieces(j):
                 if h // 2 == half:
-                    rg(d, 2, h, True).wait_recv()
-                    for j in range(S, 2, -1):
-                        if (d, h) in pieces(j):
-                            rg(d, j, h, False).start()
-                    rd(d, 2, h).start()
-        for j in [1] + list(range(3, S + 1)):
-            mixer_arrived(j)
-        for half in range(2):
-            for j in [1] + list(range(3, S + 1)):
-                for d, h in pieces(j):
-                    if h // 2 == half:
-                        rg(d, j, h, True).wait_recv()
-                        rd(d, j, h).start()
+                    rg(d, j, h, True).wait_recv()
+                    for on in range(S, j, -1):
+                        if via[half][on] == j and (d, h) in pieces(on):
+                            rg(d, on, h, False).start()
+                    rd(d, j, h).start()
+            if n == 1:
+                for m in [1] + list(range(3, S + 1)):
+                    mixer_arrived(m)
 
     @pl.when(jnp.logical_not(active))
     def _():
@@ -671,6 +665,17 @@
         settle(rout, rd_r)
 
 
+def put(a, b, out_a, out_b, same_a, same_b, sem):
+    copies = [
+        pltpu.make_async_copy(a, out_a, sem.at[0]),
+        pltpu.make_async_copy(b, out_b, sem.at[1]),
+    ]
+    for one in copies:
+        one.start()
+    for one in copies:
+        one.wait()
+
+
 def on_device(E, Y, mrows, mgain, win, wgi, wgo, taps, wmo, rrows, rgain, ids, rw, eg, eu, ed):
     M, D = mrows.shape
     T = rrows.shape[0]
@@ -687,7 +692,7 @@
     VM = pl.BlockSpec(memory_space=pltpu.VMEM)
     HB = pl.BlockSpec(memory_space=pl.ANY)
     DS = pltpu.SemaphoreType.DMA
-    return pl.pallas_call(
+    results = pl.pallas_call(
         functools.partial(kernel, E, Y, X, CAP),
         out_shape=(pltpu.VMEM((M, D), BF), pltpu.VMEM((T, D), BF)),
         in_specs=[HB] * 14,
@@ -773,6 +778,19 @@
         eu,
         ed,
     )
+    return pl.pallas_call(
+        put,
+        out_shape=(
+            jax.ShapeDtypeStruct((M, D), BF),
+            jax.ShapeDtypeStruct((T, D), BF),
+            pltpu.VMEM((M, D), BF),
+            pltpu.VMEM((T, D), BF),
+        ),
+        in_specs=[VM, VM],
+        out_specs=(HB, HB, VM, VM),
+        scratch_shapes=[DS((2,))],
+        input_output_aliases={0: 2, 1: 3},
+    )(*results)[:2]
 
 
 def solution(mesh):

time: 83.3 us -> 82.3 us (0.988)
  local copies, waits for them, and re-layouts: 1.77 us -> 0 us
    unnamed x2 -> x0, local copies, waits for them, and re-layouts: 1.77 us -> none
    pallas_call x0 -> x1, Pallas kernels: none -> 1.16 us  [on_device(): pl.pallas_call(put, out_shape=(jax.ShapeDtypeStruct((M, D), BF), jax.Shap...]
where the time goes in v5:
time: 82.3 us; the launch traced here: 82 us
  Pallas kernels  81.3 us (99%)
    pallas_call x1, Pallas kernels, on_device(): pl.pallas_call(functools.partial(kernel, E, Y, X, CAP), out_shape=(pltpu....  80.2 us

profile of v5, /device:TPU:1, one launch (start us, length us, event | category | flops | bytes accessed | tf_op | source)
XLA Modules:
  0.0 82.0 jit_solution(15283550266657116518)
XLA Ops:
  0.6 80.2 %shard_map.149 = (bf16[128,2048]{1,0:T(8,128)(2,1)S(1)}, bf16[256,2048]{1,0:T(8,128)(2,1)S(1)}) custom-call(bf16[128,2048]{1,0:T(8,128)(2,1)} %mrows_hbm.1, f32[1,2048]{1,0:T(1,128)} %bitcast.10, bf16[64,2048]{1,0:T(8,128)(2,1)} %bitcast.7, bf16[64,2048]{1,0:T(8,128)(2,1)} %bitcast.8, bf16[64,2048]{1,0:T(8,128)(2,1)} %bitcast.9, f32[3,64]{1,0:T(4,128)} %taps_hbm.1, ...), custom_call_target="tpu_custom_call" | custom-call | tf_op jit(solution)/shard_map/pallas_call | solution.py:695
  80.8 1.2 %shard_map.150 = (bf16[128,2048]{1,0:T(8,128)(2,1)}, bf16[256,2048]{1,0:T(8,128)(2,1)}, bf16[128,2048]{1,0:T(8,128)(2,1)S(1)}, bf16[256,2048]{1,0:T(8,128)(2,1)S(1)}) custom-call(bf16[128,2048]{1,0:T(8,128)(2,1)S(1)} %get-tuple-element.6.a, bf16[256,2048]{1,0:T(8,128)(2,1)S(1)} %get-tuple-element.7.b), custom_call_target="tpu_custom_call", output_to_operand_aliasing={{2}: (0, {}), {3}: (1, {})} | custom-call | tf_op jit(solution)/shard_map/pallas_call | solution.py:781

commit v6 on v5

--- a/solution.py
+++ b/solution.py
@@ -154,7 +154,9 @@
 
     FW = eg_hbm.shape[2]
     loads = [
-        pltpu.make_async_copy(rrows_hbm, rrows, l_sem.at[0]),
+        pltpu.make_async_copy(
+            rrows_hbm.at[pl.ds(0, T // 2), :], rrows.at[pl.ds(0, T // 2), :], l_sem.at[0]
+        ),
         pltpu.make_async_copy(mrows_hbm, mrows, l_sem.at[1]),
         pltpu.make_async_copy(win_hbm, win, l_sem.at[2]),
         pltpu.make_async_copy(wgi_hbm, wgi, l_sem.at[3]),
@@ -168,8 +170,11 @@
         pltpu.make_async_copy(rgain_hbm, rgain, l_sem.at[11]),
         pltpu.make_async_copy(mgain_hbm, mgain, l_sem.at[12]),
         pltpu.make_async_copy(taps_hbm, taps, l_sem.at[13]),
+        pltpu.make_async_copy(
+            rrows_hbm.at[pl.ds(T // 2, T // 2), :], rrows.at[pl.ds(T // 2, T // 2), :], l_sem.at[14]
+        ),
     ]
-    for i in (9, 0, 11):
+    for i in (9, 0, 11, 14):
         loads[i].start()
 
     barrier = pltpu.get_barrier_semaphore()
@@ -227,7 +232,9 @@
             nrm[rows, :] = (part * scale * rgain[:, cols_y]).astype(BF)
             return carry
 
-        lax.fori_loop(0, T // step, body, 0)
+        lax.fori_loop(0, T // step // 2, body, 0)
+        loads[14].wait()
+        lax.fori_loop(T // step // 2, T // step, body, 0)
 
     loads[9].wait()
 
@@ -281,7 +288,7 @@
 
     @pl.when(jnp.logical_not(active))
     def _():
-        for i in (0, 10, 11):
+        for i in (0, 10, 11, 14):
             loads[i].wait()
 
     pl.semaphore_wait(barrier, E + 2)
@@ -736,7 +743,7 @@
             pltpu.VMEM((M, 128), F32),
             pltpu.VMEM((M, 128), BF),
             pltpu.VMEM((M // 2, 128), BF),
-            DS((14,)),
+            DS((15,)),
             DS((4,)),
             DS((4,)),
             DS((2,)),

time: 82.3 us -> 81.9 us (level)
  no operation moved by 1% of the time
where the time goes in v6:
time: 81.9 us; the launch traced here: 81.8 us
  Pallas kernels  81.1 us (99%)
    pallas_call x1, Pallas kernels, on_device(): pl.pallas_call(functools.partial(kernel, E, Y, X, CAP), out_shape=(pltpu....  80 us

profile of v6, /device:TPU:1, one launch (start us, length us, event | category | flops | bytes accessed | tf_op | source)
XLA Modules:
  0.0 81.8 jit_solution(12246219383601789119)
XLA Ops:
  0.6 80.0 %shard_map.149 = (bf16[128,2048]{1,0:T(8,128)(2,1)S(1)}, bf16[256,2048]{1,0:T(8,128)(2,1)S(1)}) custom-call(bf16[128,2048]{1,0:T(8,128)(2,1)} %mrows_hbm.1, f32[1,2048]{1,0:T(1,128)} %bitcast.10, bf16[64,2048]{1,0:T(8,128)(2,1)} %bitcast.7, bf16[64,2048]{1,0:T(8,128)(2,1)} %bitcast.8, bf16[64,2048]{1,0:T(8,128)(2,1)} %bitcast.9, f32[3,64]{1,0:T(4,128)} %taps_hbm.1, ...), custom_call_target="tpu_custom_call" | custom-call | tf_op jit(solution)/shard_map/pallas_call | solution.py:702
  80.6 1.2 %shard_map.150 = (bf16[128,2048]{1,0:T(8,128)(2,1)}, bf16[256,2048]{1,0:T(8,128)(2,1)}, bf16[128,2048]{1,0:T(8,128)(2,1)S(1)}, bf16[256,2048]{1,0:T(8,128)(2,1)S(1)}) custom-call(bf16[128,2048]{1,0:T(8,128)(2,1)S(1)} %get-tuple-element.6.a, bf16[256,2048]{1,0:T(8,128)(2,1)S(1)} %get-tuple-element.7.b), custom_call_target="tpu_custom_call", output_to_operand_aliasing={{2}: (0, {}), {3}: (1, {})} | custom-call | tf_op jit(solution)/shard_map/pallas_call | solution.py:788
